TPU v7x, 256 devices: a whole 4x4x8 slice. The times are simulated.
256 devices in a mesh: sp: 32 (over z, y), tp: 8 (over x, core).
Axes of the slice: x: 4, y: 4, z: 8, core: 2. Of those that a mesh axis runs over, the one named last changes fastest.
Arguments:
- stream: bfloat16 [24576, 2048], P(('sp', 'tp')), may hold values from -6 to 6
- query_first: bfloat16 [24576, 1024], P('sp', 'tp'), may hold values from -6 to 6
- key_first: bfloat16 [24576, 1024], P('sp', 'tp'), may hold values from -6 to 6
- value_first: bfloat16 [24576, 1024], P('sp', 'tp'), may hold values from -6 to 6
- decay_first: bfloat16 [24576, 1024], P('sp', 'tp'), may hold values from -16 to 1
- learning_first: bfloat16 [24576, 1024], P('sp', 'tp'), may hold values from -16 to 4
- output_gate_first: bfloat16 [24576, 1024], P('sp', 'tp'), may hold values from -6 to 6
- extra_decay_first: float32 [24576, 16], P('sp', 'tp'), may hold values from -1 to 0
- head_norm_gain_first: float32 [1024], P('tp'), may hold values from 0.1 to 1.9
- self_weight_first: float32 [1024], P('tp'), may hold values from -0.9 to 0.9
- query_second: bfloat16 [24576, 1024], P('sp', 'tp'), may hold values from -6 to 6
- key_second: bfloat16 [24576, 1024], P('sp', 'tp'), may hold values from -6 to 6
- value_second: bfloat16 [24576, 1024], P('sp', 'tp'), may hold values from -6 to 6
- decay_second: bfloat16 [24576, 1024], P('sp', 'tp'), may hold values from -16 to 1
- learning_second: bfloat16 [24576, 1024], P('sp', 'tp'), may hold values from -16 to 4
- output_gate_second: bfloat16 [24576, 1024], P('sp', 'tp'), may hold values from -6 to 6
- extra_decay_second: float32 [24576, 8], P('sp', 'tp'), may hold values from -1 to 0
- head_norm_gain_second: float32 [1024], P('tp'), may hold values from 0.1 to 1.9
- self_weight_second: float32 [1024], P('tp'), may hold values from -0.9 to 0.9
- output_projection_first: bfloat16 [1024, 2048], replicated, may hold values from -0.125 to 0.125
- output_projection_second: bfloat16 [1024, 2048], replicated, may hold values from -0.125 to 0.125
- middle_norm_gain: float32 [2048], replicated, may hold values from 0.1 to 1.9
- mixer_up_weight: bfloat16 [2048, 8192], P('sp', 'tp'), may hold values from -0.125 to 0.125
- mixer_down_weight: bfloat16 [8192, 2048], P('tp', 'sp'), may hold values from -0.0625 to 0.0625
- final_norm_gain: float32 [2048], replicated, may hold values from 0.1 to 1.9
Outputs:
- result: bfloat16 [24576, 2048], P(('sp', 'tp'))
All inputs are finite; a program needn't handle non-finite values.
Results may differ from a plain program's by a relative error of at most 0.019.
Values may be sent and summed in bfloat16 or wider, within the bound.
No kernel may reach another device: no remote copies, remote signals or barrier semaphores. Data moves between devices by JAX's collectives and lax.ppermute only.
A program may use at most 128 MiB of HBM per device.

v0:
```python
import jax
import jax.numpy as jnp
from jax import lax
from jax.experimental import pallas as pl
from jax.experimental.pallas import tpu as pltpu
from jax.sharding import Mesh
from jax.sharding import PartitionSpec as P

CHUNK = 64
LANES = 128
FIRST_HEAD_SIZE = 64
SECOND_HEAD_SIZE = 128
SP = ("z", "y")
TP = ("x", "c")
ALL = ("z", "y", "x", "c")
EPS_KEY = 1e-05
EPS_HEAD = 0.00064
EPS_NORM = 1e-05
ALPHA = 2.0**0.25
F32 = jnp.float32
BF16 = jnp.bfloat16


def mm(a, b):
    return jnp.dot(a.astype(BF16), b.astype(BF16), preferred_element_type=F32)


def mm_nt(a, b):
    return lax.dot_general(
        a.astype(BF16), b.astype(BF16), (((1,), (1,)), ((), ())), preferred_element_type=F32
    )


def mm_tn(a, b):
    return lax.dot_general(
        a.astype(BF16), b.astype(BF16), (((0,), (0,)), ((), ())), preferred_element_type=F32
    )


def iotas(rows=LANES, cols=LANES):
    return (
        lax.broadcasted_iota(jnp.int32, (rows, cols), 0),
        lax.broadcasted_iota(jnp.int32, (rows, cols), 1),
    )


def halves(rows):
    return lax.broadcasted_iota(jnp.int32, (rows, LANES), 1) < FIRST_HEAD_SIZE


def head_mean(array, pair):
    if not pair:
        return jnp.mean(array, -1, keepdims=True)
    low = halves(array.shape[0])
    first = jnp.sum(jnp.where(low, array, 0.0), -1, keepdims=True)
    second = jnp.sum(jnp.where(low, 0.0, array), -1, keepdims=True)
    return jnp.where(low, first, second) / FIRST_HEAD_SIZE


def spread(array):
    low = halves(array.shape[0])
    return jnp.concatenate([jnp.where(low, array, 0.0), jnp.where(low, 0.0, array)], 0)


def features(q_ref, k_ref, v_ref, d_ref, l_ref, e_ref, pair):
    q, k, v = (r[...].astype(F32) for r in (q_ref, k_ref, v_ref))
    size = FIRST_HEAD_SIZE if pair else SECOND_HEAD_SIZE
    normed = k * lax.rsqrt(head_mean(k * k, pair) + EPS_KEY) * size ** (-0.5)
    learn = jax.nn.sigmoid(l_ref[...].astype(F32))
    burst = e_ref[...]
    if pair:
        burst = jnp.where(halves(q.shape[0]), burst[:, 0:1], burst[:, 1:2])
    logdec = jax.nn.sigmoid(d_ref[...].astype(F32)) * (-(2.718281828459045**-0.5)) + burst
    return q, k, v, normed, learn, logdec


def running_sum(logdec):
    rows, cols = iotas()
    tri = ((rows // CHUNK == cols // CHUNK) & (cols <= rows)).astype(BF16)
    high = logdec.astype(BF16)
    rest = logdec - high.astype(F32)
    mid = rest.astype(BF16)
    low = (rest - mid.astype(F32)).astype(BF16)
    return mm(tri, high) + (mm(tri, mid) + mm(tri, low))


def chunk_row(array, at):
    return jnp.concatenate(
        [
            jnp.broadcast_to(array[c * CHUNK + at : c * CHUNK + at + 1], (CHUNK, array.shape[1]))
            for c in range(array.shape[0] // CHUNK)
        ],
        0,
    )


def inverses(lowers):
    rows, cols = iotas()
    eye = (rows == cols).astype(F32)
    found = [eye + jnp.where(rows // 2 == cols // 2, low, 0.0) for low in lowers]
    step = 2
    while step < CHUNK:
        mask = (rows // (2 * step) == cols // (2 * step)) & (rows // step != cols // step)
        short = [x.astype(BF16) for x in found]
        part = [mm(x, jnp.where(mask, low, 0.0)) for x, low in zip(short, lowers)]
        found = [f + mm(p, x) for f, p, x in zip(found, part, short)]
        step *= 2
    return found


def maps_kernel(*refs):
    ins, outs, carry = refs[:12], refs[12:21], refs[21]
    step = pl.program_id(0)
    rows, cols = iotas()
    same = rows // CHUNK == cols // CHUNK
    strict = same & (cols < rows)
    inclusive = same & (cols <= rows)
    eye = (rows == cols).astype(F32)

    @pl.when(step == 0)
    def _():
        for g in range(2):
            carry[g, :LANES, :] = eye
            carry[g, LANES:, :] = jnp.zeros((LANES, LANES), F32)

    units = []
    keeps = []
    for g in range(2):
        q, k, v, normed, learn, logdec = features(*ins[6 * g : 6 * g + 6], g == 0)
        forward, backward = -normed, normed * learn
        cumul = running_sum(logdec)
        before = cumul - logdec
        middle = chunk_row(cumul, CHUNK // 2)
        ending = chunk_row(cumul, CHUNK - 1)
        up, down, left = jnp.exp(before - middle), jnp.exp(middle - cumul), jnp.exp(ending - cumul)
        keeps.append([jnp.exp(cumul[c * CHUNK + CHUNK - 1 : (c + 1) * CHUNK]) for c in range(2)])
        parts = (
            forward * up,
            q * jnp.exp(cumul - middle),
            backward * down,
            k * down,
            forward * jnp.exp(before),
            q * jnp.exp(cumul),
            backward * left,
            k * left,
            v,
        )
        if g == 0:
            for c in range(2):
                units.append([spread(p[c * CHUNK : (c + 1) * CHUNK]) for p in parts])
        else:
            units.append(list(parts))
    units = [[p.astype(BF16) for p in u[:5]] + [u[5]] + [p.astype(BF16) for p in u[6:]] for u in units]
    grams = [
        mm_nt(jnp.concatenate([u[0], u[1]], 0), jnp.concatenate([u[2], u[3]], 0)) for u in units
    ]
    lowers = [jnp.where(strict, m[:LANES, :LANES], 0.0) for m in grams]
    writes = [jnp.where(strict, m[:LANES, LANES:], 0.0) for m in grams]
    read_corr = [jnp.where(inclusive, m[LANES:, :LANES], 0.0) for m in grams]
    read_write = [jnp.where(inclusive, m[LANES:, LANES:], 0.0) for m in grams]
    solvers = inverses(lowers)
    sides = [
        jnp.concatenate([u[4], mm(w, u[8]).astype(BF16)], 1) for u, w in zip(units, writes)
    ]
    solved = [mm(x, s).astype(BF16) for x, s in zip(solvers, sides)]
    carried = [mm(r, s) for r, s in zip(read_corr, solved)]
    entry = [u[5] + c[:, :LANES] for u, c in zip(units, carried)]
    inner = [c[:, LANES:] + mm(r, u[8]) for u, c, r in zip(units, carried, read_write)]
    moved = []
    for n, (u, s) in enumerate(zip(units, solved)):
        for c in range(1 if n < 2 else 2):
            at = slice(0, LANES) if n < 2 else slice(c * CHUNK, (c + 1) * CHUNK)
            both = mm_tn(s[at], u[6][at])
            moved.append((both[:LANES], both[LANES:] + mm_tn(u[8][at], u[7][at])))
    entry_1, inner_1, entry_2, inner_2, starts_q1, starts_z1, starts_q2, starts_z2, total = outs
    for c in range(2):
        at = slice(c * CHUNK, (c + 1) * CHUNK)
        entry_1[at] = (entry[c][:CHUNK] + entry[c][CHUNK:]).astype(BF16)
        inner_1[at] = inner[c][:CHUNK] + inner[c][CHUNK:]
    entry_2[...] = entry[2].astype(BF16)
    inner_2[...] = inner[2]
    held = [carry[0], carry[1]]
    for c in range(2):
        for g, (sq, sz) in enumerate(((starts_q1, starts_z1), (starts_q2, starts_z2))):
            sq[c] = held[g][:LANES].astype(BF16)
            sz[c] = held[g][LANES:]
            transit, update = moved[2 * g + c]
            after = held[g] * keeps[g][c] + mm(held[g], transit)
            held[g] = jnp.concatenate([after[:LANES], after[LANES:] + update], 0)
    for g in range(2):
        carry[g] = held[g]

    @pl.when(step == pl.num_programs(0) - 1)
    def _():
        first, second = held
        total[0:64] = (first[0:64] + first[64:128]).astype(BF16)
        total[64:128] = (first[128:192] + first[192:256]).astype(BF16)
        total[128:384] = second.astype(BF16)


def chunk_maps(first, second):
    tokens = first[0].shape[0]
    steps = tokens // LANES
    chunks = tokens // CHUNK

    def rows(width=LANES):
        return pl.BlockSpec((LANES, width), lambda i: (i, 0))

    state = pl.BlockSpec((2, LANES, LANES), lambda i: (i, 0, 0))
    ins = []
    for group in (first, second):
        ins += [rows()] * 5 + [rows(group[5].shape[1])]
    return pl.pallas_call(
        maps_kernel,
        grid=(steps,),
        in_specs=ins,
        out_specs=[rows()] * 4 + [state] * 4 + [pl.BlockSpec((384, LANES), lambda i: (0, 0))],
        out_shape=[
            jax.ShapeDtypeStruct((tokens, LANES), t) for t in (BF16, F32, BF16, F32)
        ]
        + [jax.ShapeDtypeStruct((chunks, LANES, LANES), t) for t in (BF16, F32, BF16, F32)]
        + [jax.ShapeDtypeStruct((384, LANES), BF16)],
        scratch_shapes=[pltpu.VMEM((2, 2 * LANES, LANES), F32)],
        cost_estimate=pl.CostEstimate(
            flops=12_000_000_000, bytes_accessed=8_000_000, transcendentals=2_000_000
        ),
        name="chunk_maps",
    )(*first, *second)


def unpack(packed):
    def widen(part):
        return spread(part.astype(F32))

    return (
        jnp.concatenate([widen(packed[0:64]), widen(packed[64:128])], 0),
        packed[128:384].astype(F32),
    )


def pack(pairs):
    first, second = pairs
    return jnp.concatenate(
        [first[0:64] + first[64:128], first[128:192] + first[192:256], second], 0
    )


def compose(earlier, later):
    out = []
    for a, b in zip(earlier, later):
        moved = mm(a, b[:LANES])
        out.append(jnp.concatenate([moved[:LANES], moved[LANES:] + b[LANES:]], 0))
    return out


def row_kernel(mine_ref, own, one, two, three, before_ref, total_ref):
    mine = mine_ref[0]
    by_shift = [r[...] for r in (own, one, two, three)]

    def member(k):
        shift = lax.rem(mine - k + 4, 4)
        out = by_shift[3]
        for s in range(3):
            out = jnp.where(shift == s, by_shift[s], out)
        return unpack(out)

    rows, cols = iotas()
    eye = (rows == cols).astype(F32)
    neutral = jnp.concatenate([eye, jnp.zeros((LANES, LANES), F32)], 0)
    running = member(0)
    before = [jnp.where(mine == 0, neutral, r) for r in running]
    for k in range(1, 4):
        before = [jnp.where(mine == k, r, b) for r, b in zip(running, before)] if k > 1 else [
            jnp.where(mine == 0, neutral, r) for r in running
        ]
        running = compose(running, member(k))
    before_ref[...] = pack(before)
    total_ref[...] = pack(running)


def vmem_call(kernel, out_shape, *args, scalars=0, name=None):
    return pl.pallas_call(
        kernel,
        in_specs=[pl.BlockSpec(memory_space=pltpu.SMEM)] * scalars
        + [pl.BlockSpec(memory_space=pltpu.VMEM)] * (len(args) - scalars),
        out_specs=jax.tree.map(lambda _: pl.BlockSpec(memory_space=pltpu.VMEM), out_shape),
        out_shape=out_shape,
        name=name,
    )(*args)


def join_kernel(earlier_ref, later_ref, out_ref):
    out_ref[...] = pack(compose(unpack(earlier_ref[...]), unpack(later_ref[...])))


def join_two_kernel(earlier_ref, before_ref, through_ref, before_out, through_out):
    earlier = unpack(earlier_ref[...])
    before_out[...] = pack(compose(earlier, unpack(before_ref[...])))
    through_out[...] = pack(compose(earlier, unpack(through_ref[...])))


def shift(array, axis, by, size, wrap):
    pairs = [(i, (i + by) % size) for i in range(size) if wrap or 0 <= i + by < size]
    return lax.ppermute(array, axis, pairs)


def sequence_prefix(total):
    shape = jax.ShapeDtypeStruct(total.shape, F32)
    ny, nz = lax.axis_size("y"), lax.axis_size("z")
    peers = [shift(total, "y", s, ny, True) for s in (1, 2, 3)]
    mine = lax.axis_index("y").astype(jnp.int32).reshape(1)
    row_before, row_total = vmem_call(
        row_kernel, (shape, shape), mine, total, *peers, scalars=1, name="row_maps"
    )
    before = shift(row_total.astype(BF16), "z", 1, nz, False)
    through = vmem_call(join_kernel, shape, before, row_total, name="join_one")
    earlier = shift(through.astype(BF16), "z", 2, nz, False)
    before, through = vmem_call(
        join_two_kernel, (shape, shape), earlier, before, through, name="join_two"
    )
    send = jnp.concatenate([through[64:128], through[256:384]], 0).astype(BF16)
    last = shift(send, "z", 4, nz, False)
    return last, before, row_before


def outputs_kernel(*refs):
    (last, before, row_before), ins, out, states = refs[:3], refs[3:19], refs[19], refs[20]

    @pl.when(pl.program_id(0) == 0)
    def _():
        near = unpack(before[...])
        row = unpack(row_before[...])
        far = (spread(last[0:64].astype(F32)), last[64:192])
        for g in range(2):
            start = mm(far[g], near[g][:LANES]) + near[g][LANES:]
            states[g] = mm(start, row[g][:LANES]) + row[g][LANES:]

    for g in range(2):
        entry, inner, sq, sz, q_ref, k_ref, v_ref, gate_ref = ins[8 * g : 8 * g + 8]
        pair = g == 0
        gain, weight = out_params(refs, g)
        start = states[g].astype(BF16)
        pieces = []
        for c in range(2):
            at = slice(c * CHUNK, (c + 1) * CHUNK)
            state = mm(start, sq[c]) + sz[c]
            pieces.append(mm_nt(entry[at], state) + inner[at])
        heady = jnp.concatenate(pieces, 0)
        q, k, v, gate = (r[...].astype(F32) for r in (q_ref, k_ref, v_ref, gate_ref))
        centred = heady - head_mean(heady, pair)
        spread_ = head_mean(centred * centred, pair)
        normalized = centred * lax.rsqrt(spread_ + EPS_HEAD) * gain
        size = FIRST_HEAD_SIZE if pair else SECOND_HEAD_SIZE
        extra = head_mean(q * k * weight, pair) * size * v
        out[:, g * LANES : (g + 1) * LANES] = (
            (normalized + extra) * jax.nn.sigmoid(gate)
        ).astype(BF16)


def out_params(refs, g):
    params = refs[21]
    return params[2 * g : 2 * g + 1], params[2 * g + 1 : 2 * g + 2]


def mixer_outputs(prefix, groups, params):
    tokens = groups[0][0].shape[0]
    rows = pl.BlockSpec((LANES, LANES), lambda i: (i, 0))
    state = pl.BlockSpec((2, LANES, LANES), lambda i: (i, 0, 0))

    def whole(a):
        return pl.BlockSpec(a.shape, lambda i: (0,) * a.ndim)

    def kernel(*refs):
        ins, out, states = refs[:20], refs[20], refs[21]
        outputs_kernel(*ins[:19], out, states, ins[19])

    return pl.pallas_call(
        kernel,
        grid=(tokens // LANES,),
        in_specs=[whole(a) for a in prefix]
        + [rows, rows, state, state, rows, rows, rows, rows] * 2
        + [whole(params)],
        out_specs=pl.BlockSpec((LANES, 2 * LANES), lambda i: (i, 0)),
        out_shape=jax.ShapeDtypeStruct((tokens, 2 * LANES), BF16),
        scratch_shapes=[pltpu.VMEM((2, LANES, LANES), F32)],
        cost_estimate=pl.CostEstimate(
            flops=2_000_000_000, bytes_accessed=6_000_000, transcendentals=300_000
        ),
        name="mixer_outputs",
    )(*prefix, *groups[0], *groups[1], params)


def norm_rows(array, gain):
    mean_part = jnp.mean(array, -1, keepdims=True)
    centred = array - mean_part
    return centred * lax.rsqrt(jnp.mean(centred * centred, -1, keepdims=True) + EPS_NORM) * gain


def project_kernel(rows_ref, first_ref, second_ref, stream_ref, gain_ref, out_ref, acc):
    step = pl.program_id(0)
    rows = rows_ref[0]

    @pl.when(step == 0)
    def _():
        acc[...] = ALPHA * stream_ref[...].astype(F32)

    acc[...] += jnp.dot(rows[:, :LANES], first_ref[...], preferred_element_type=F32) + jnp.dot(
        rows[:, LANES:], second_ref[...], preferred_element_type=F32
    )

    @pl.when(step == pl.num_programs(0) - 1)
    def _():
        out_ref[...] = norm_rows(acc[...], gain_ref[...]).astype(BF16)


def project(rows, first, second, stream, gain):
    peers, count, _ = rows.shape
    width = first.shape[1]
    weight = pl.BlockSpec((LANES, width), lambda i: (i, 0))
    return pl.pallas_call(
        project_kernel,
        grid=(peers,),
        in_specs=[
            pl.BlockSpec((1, count, 2 * LANES), lambda i: (i, 0, 0)),
            weight,
            weight,
            pl.BlockSpec((count, width), lambda i: (0, 0)),
            pl.BlockSpec((1, width), lambda i: (0, 0)),
        ],
        out_specs=pl.BlockSpec((count, width), lambda i: (0, 0)),
        out_shape=jax.ShapeDtypeStruct((count, width), BF16),
        scratch_shapes=[pltpu.VMEM((count, width), F32)],
        cost_estimate=pl.CostEstimate(
            flops=4_000_000_000, bytes_accessed=9_000_000, transcendentals=100
        ),
        name="project",
    )(rows, first, second, stream, gain.reshape(1, -1))


def swap_core(array):
    return lax.ppermute(array, "c", [(0, 1), (1, 0)])


def local(
    stream,
    query_first,
    key_first,
    value_first,
    decay_first,
    learning_first,
    output_gate_first,
    extra_decay_first,
    head_norm_gain_first,
    self_weight_first,
    query_second,
    key_second,
    value_second,
    decay_second,
    learning_second,
    output_gate_second,
    extra_decay_second,
    head_norm_gain_second,
    self_weight_second,
    output_projection_first,
    output_projection_second,
    middle_norm_gain,
    mixer_up_weight,
    mixer_down_weight,
    final_norm_gain,
):
    count, width = stream.shape
    depth = mixer_up_weight.shape[0]
    hidden_width = mixer_up_weight.shape[1]
    both = jnp.concatenate([mixer_up_weight, mixer_down_weight.T], 0)
    weights = lax.all_gather(both, SP)
    up_whole = weights[:, :depth].reshape(-1, hidden_width)
    down_whole = weights[:, depth:].reshape(-1, hidden_width)

    maps = chunk_maps(
        (query_first, key_first, value_first, decay_first, learning_first, extra_decay_first),
        (query_second, key_second, value_second, decay_second, learning_second, extra_decay_second),
    )
    entry_1, inner_1, entry_2, inner_2, sq1, sz1, sq2, sz2, total = maps
    prefix = sequence_prefix(total)
    params = jnp.stack(
        [head_norm_gain_first, self_weight_first, head_norm_gain_second, self_weight_second]
    )
    mixer = mixer_outputs(
        prefix,
        (
            (entry_1, inner_1, sq1, sz1, query_first, key_first, value_first, output_gate_first),
            (entry_2, inner_2, sq2, sz2, query_second, key_second, value_second, output_gate_second),
        ),
        params,
    )
    rows = lax.all_to_all(mixer.reshape(-1, count, 2 * LANES), TP, 0, 0, tiled=True)
    middle = project(
        rows, output_projection_first, output_projection_second, stream, middle_norm_gain
    )

    nx = lax.axis_size("x")
    half = count // 2
    near_p = shift(middle, "x", 1, nx, True)
    near_m = shift(middle, "x", -1, nx, True)
    far_p = shift(near_p[:half], "x", 1, nx, True)
    far_m = shift(near_m[half:], "x", -1, nx, True)
    far = jnp.concatenate([far_p, far_m], 0)

    def channel(block):
        rows_all = jnp.concatenate([block, swap_core(block)], 0)
        upward = jnp.dot(rows_all, up_whole, preferred_element_type=F32)
        hidden = jnp.square(jax.nn.relu(upward)).astype(BF16)
        part = lax.dot_general(
            hidden, down_whole, (((1,), (1,)), ((), ())), preferred_element_type=F32
        ).astype(BF16)
        size = block.shape[0]
        return part[:size].astype(F32) + swap_core(part[size:]).astype(F32)

    sum_own = channel(middle)
    sum_near = channel(jnp.concatenate([near_p, near_m], 0))
    sum_far = channel(far)
    sum_p, sum_m = sum_near[:count], sum_near[count:]
    from_p = shift(sum_far[:half].astype(BF16), "x", 1, nx, True).astype(F32)
    from_m = shift(sum_far[half:].astype(BF16), "x", -1, nx, True).astype(F32)
    sum_m = jnp.concatenate([sum_m[:half] + from_p, sum_m[half:]], 0).astype(BF16)
    sum_p = jnp.concatenate([sum_p[:half], sum_p[half:] + from_m], 0).astype(BF16)
    ff_total = (
        sum_own
        + shift(sum_p, "x", -1, nx, True).astype(F32)
        + shift(sum_m, "x", 1, nx, True).astype(F32)
    )
    return norm_rows(ALPHA * middle.astype(F32) + ff_total, final_norm_gain).astype(BF16)


def solution(mesh):
    split = Mesh(mesh.devices.reshape(8, 4, 4, 2), ALL)
    long = P(SP, TP)
    group = (long,) * 7 + (P(TP), P(TP))
    return jax.shard_map(
        local,
        mesh=split,
        in_specs=(P(ALL, None),)
        + group
        + group
        + (P(), P(), P(), P(SP, TP), P(TP, SP), P()),
        out_specs=P(ALL, None),
        check_vma=False,
    )
```

profile of v0, /device:TPU:16, one launch (start us, length us, event | category | flops | bytes accessed | tf_op | source)
XLA Modules:
  0.0 186.4 jit_solution(10500907074114250468)
XLA Ops:
  6.5 1.7 pad_maximum_fusion.4
  8.2 1.6 copy.26.refs_5_
  9.9 1.6 copy.27.refs_11_
  11.5 17.4 %chunk_maps.1 = (bf16[768,128]{1,0:T(8,128)(2,1)}, f32[768,128]{1,0:T(8,128)}, bf16[768,128]{1,0:T(8,128)(2,1)}, f32[768,128]{1,0:T(8,128)}, bf16[12,128,128]{2,...) custom-call(bf16[768,128]{1,0:T(8,128)(2,1)} %refs_7_.3, ...), custom_call_target="tpu_custom_call" | custom-call | flops 12000000000 | bytes 8000000 | tf_op jit(solution)/shard_map/chunk_maps/pallas_call | solution.py:213
  31.1 2.5 %collective-permute-start.2 = (bf16[384,128]{1,0:T(8,128)(2,1)}, bf16[384,128]{1,0:T(8,128)(2,1)S(1)}, u32[]{:S(2)}, u32[]{:S(2)}) collective-permute-start(bf16[384,128]{1,0:T(8,128)(2,1)} %get-tuple-element.18.own), channel_id=1, source_target_pairs={{0,24},{8,0},{16,8},{24,16},{1,25},{9,1},{17,9},{25,17},{2,26},{10... | collective-permute-start | bytes 294920 | tf_op jit(solution)/shard_map/ppermute | solution.py:304
  33.7 1.5 collective-permute-done.one
  35.2 1.8 collective-permute-done.1.two
  37.0 2.0 %collective-permute-done.2.three = bf16[384,128]{1,0:T(8,128)(2,1)S(1)} collective-permute-done((bf16[384,128]{1,0:T(8,128)(2,1)}, bf16[384,128]{1,0:T(8,128)(2,1)S(1)}, u32[]{:S(2)}, u32[]{:S(2)}) %collective-permute-start.2) | collective-permute-done | bytes 98336 | tf_op jit(solution)/shard_map/ppermute | solution.py:304
  39.7 2.2 %row_maps.1 = (f32[384,128]{1,0:T(8,128)}, f32[384,128]{1,0:T(8,128)}) custom-call(s32[1]{0:T(128)} %bitcast.mine_ref, bf16[384,128]{1,0:T(8,128)(2,1)} %get-tuple-element.18.own, bf16[384,128]{1,0:T(8,128)(2,1)} %copy-done.3, bf16[384,128]{1,0:T(8,128)(2,1)} %copy-done.4, bf16[384,128]{1,0:T(8,128)(2,1)} %copy-done.5), custom_call_target="tpu_custom_call" | custom-call | tf_op jit(solution)/shard_map/row_maps/pallas_call | solution.py:282
  42.8 3.4 %collective-permute-start.3 = (bf16[384,128]{1,0:T(8,128)(2,1)S(1)}, bf16[384,128]{1,0:T(8,128)(2,1)S(1)}, u32[]{:S(2)}, u32[]{:S(2)}) collective-permute-start(bf16[384,128]{1,0:T(8,128)(2,1)S(1)} %convert_element_type.65), channel_id=1, source_target_pairs={{0,32},{32,64},{64,96},{96,128},{128,160},{160,192},{192,224},{1,3... | collective-permute-start | bytes 294920 | tf_op jit(solution)/shard_map/ppermute | solution.py:304
  46.2 2.3 %collective-permute-done.3.earlier_ref.before_ref = bf16[384,128]{1,0:T(8,128)(2,1)S(1)} collective-permute-done((bf16[384,128]{1,0:T(8,128)(2,1)S(1)}, bf16[384,128]{1,0:T(8,128)(2,1)S(1)}, u32[]{:S(2)}, u32[]{:S(2)}) %collective-permute-start.3) | collective-permute-done | bytes 98336 | tf_op jit(solution)/shard_map/ppermute | solution.py:304
  49.1 1.8 join_one.1.through_ref
  51.9 5.7 %collective-permute-start.4 = (bf16[384,128]{1,0:T(8,128)(2,1)S(1)}, bf16[384,128]{1,0:T(8,128)(2,1)S(1)}, u32[]{:S(2)}, u32[]{:S(2)}) collective-permute-start(bf16[384,128]{1,0:T(8,128)(2,1)S(1)} %convert_element_type.66), channel_id=1, source_target_pairs={{0,64},{32,96},{64,128},{96,160},{128,192},{160,224},{1,65},{33,97... | collective-permute-start | bytes 294920 | tf_op jit(solution)/shard_map/ppermute | solution.py:304
  57.6 2.2 %collective-permute-done.4.earlier_ref = bf16[384,128]{1,0:T(8,128)(2,1)S(1)} collective-permute-done((bf16[384,128]{1,0:T(8,128)(2,1)S(1)}, bf16[384,128]{1,0:T(8,128)(2,1)S(1)}, u32[]{:S(2)}, u32[]{:S(2)}) %collective-permute-start.4) | collective-permute-done | bytes 98336 | tf_op jit(solution)/shard_map/ppermute | solution.py:304
  60.4 1.9 %join_two.1 = (f32[384,128]{1,0:T(8,128)}, f32[384,128]{1,0:T(8,128)}) custom-call(bf16[384,128]{1,0:T(8,128)(2,1)} %copy-done.6, bf16[384,128]{1,0:T(8,128)(2,1)} %copy-done.1, f32[384,128]{1,0:T(8,128)} %join_one.1.through_ref), custom_call_target="tpu_custom_call" | custom-call | tf_op jit(solution)/shard_map/join_two/pallas_call | solution.py:282
  63.3 11.7 %collective-permute-start.5 = (bf16[192,128]{1,0:T(8,128)(2,1)S(1)}, bf16[192,128]{1,0:T(8,128)(2,1)S(1)}, u32[]{:S(2)}, u32[]{:S(2)}) collective-permute-start(bf16[192,128]{1,0:T(8,128)(2,1)S(1)} %pad_maximum_fusion.5), channel_id=1, source_target_pairs={{0,128},{32,160},{64,192},{96,224},{1,129},{33,161},{65,193},{97,2... | collective-permute-start | bytes 147464 | tf_op jit(solution)/shard_map/ppermute | solution.py:304
  77.5 7.5 %mixer_outputs.1 = bf16[768,256]{1,0:T(8,128)(2,1)} custom-call(bf16[192,128]{1,0:T(8,128)(2,1)} %copy-done.13, f32[384,128]{1,0:T(8,128)} %get-tuple-element.21.refs_1_, f32[384,128]{1,0:T(8,128)} %get-tuple-element.22.refs_2_, bf16[768,128]{1,0:T(8,128)(2,1)} %get-tuple-element.23.refs_3_, f32[768,128]{1,0:T(8,128)} %get-tuple-element.24.refs_4_, ...), custom_call_target="tpu_custom_call" | custom-call | flops 2000000000 | bytes 6000000 | tf_op jit(solution)/shard_map/mixer_outputs/pallas_call | solution.py:377
  85.0 13.3 %all_to_all.5.rows_ref = bf16[8,96,256]{2,1,0:T(8,128)(2,1)} all-to-all(bf16[8,96,256]{2,1,0:T(8,128)(2,1)} %bitcast.24), channel_id=1, replica_groups=mesh['z'=8,'y'=4,'x'=4,'c'=2] {'x','c'}, dimensions={0} | all-to-all | bytes 786432 | tf_op jit(solution)/shard_map/all_to_all | solution.py:496
  98.3 8.4 %project.1 = bf16[96,2048]{1,0:T(8,128)(2,1)} custom-call(bf16[8,96,256]{2,1,0:T(8,128)(2,1)} %all_to_all.5.rows_ref, bf16[1024,2048]{1,0:T(8,128)(2,1)} %first_ref.1, bf16[1024,2048]{1,0:T(8,128)(2,1)} %second_ref.1, bf16[96,2048]{1,0:T(8,128)(2,1)} %stream_ref.1, f32[1,2048]{1,0:T(1,128)} %bitcast.30), custom_call_target="tpu_custom_call" | custom-call | flops 4000000000 | bytes 9000000 | tf_op jit(solution)/shard_map/project/pallas_call | solution.py:420
  108.7 8.8 %collective-permute-done.9 = bf16[96,2048]{1,0:T(8,128)(2,1)S(1)} collective-permute-done((bf16[96,2048]{1,0:T(8,128)(2,1)}, bf16[96,2048]{1,0:T(8,128)(2,1)S(1)}, u32[]{:S(2)}, u32[]{:S(2)}) %collective-permute-start.9) | collective-permute-done | bytes 393248 | tf_op jit(solution)/shard_map/ppermute | solution.py:304
  117.6 2.5 %collective-permute-start.13 = (bf16[48,2048]{1,0:T(8,128)(2,1)S(1)}, bf16[48,2048]{1,0:T(8,128)(2,1)S(1)}, u32[]{:S(2)}, u32[]{:S(2)}) collective-permute-start(bf16[48,2048]{1,0:T(8,128)(2,1)S(1)} %slice.95), channel_id=1, source_target_pairs={{0,6},{2,0},{4,2},{6,4},{1,7},{3,1},{5,3},{7,5},{8,14},{10,8},{12,... | collective-permute-start | bytes 589832 | tf_op jit(solution)/shard_map/ppermute | solution.py:304
  120.9 2.4 %collective-permute-done.13 = bf16[48,2048]{1,0:T(8,128)(2,1)S(1)} collective-permute-done((bf16[48,2048]{1,0:T(8,128)(2,1)S(1)}, bf16[48,2048]{1,0:T(8,128)(2,1)S(1)}, u32[]{:S(2)}, u32[]{:S(2)}) %collective-permute-start.13) | collective-permute-done | bytes 196640 | tf_op jit(solution)/shard_map/ppermute | solution.py:304
  123.3 3.8 %collective-permute-done.12 = bf16[48,2048]{1,0:T(8,128)(2,1)S(1)} collective-permute-done((bf16[48,2048]{1,0:T(8,128)(2,1)S(1)}, bf16[48,2048]{1,0:T(8,128)(2,1)S(1)}, u32[]{:S(2)}, u32[]{:S(2)}) %collective-permute-start.12) | collective-permute-done | bytes 196640 | tf_op jit(solution)/shard_map/ppermute | solution.py:304
  127.4 6.2 %fusion.41 = (bf16[32,64,1024]{2,1,0:T(8,128)(2,1)}, bf16[32,64,1024]{2,1,0:T(8,128)(2,1)}) fusion(bf16[32,128,1024]{2,1,0:T(8,128)(2,1)} %bitcast.17), kind=kLoop, calls=%fused_computation.52 | loop fusion | bytes 16777216 | tf_op jit(solution)/shard_map/slice | solution.py:476
  134.5 7.1 %convolution_convert_fusion = bf16[384,2048]{1,0:T(8,128)(2,1)S(1)} fusion(bf16[2048,1024]{1,0:T(8,128)(2,1)} %bitcast.21, bf16[2048,1024]{1,0:T(8,128)(2,1)} %bitcast.18, bf16[192,2048]{1,0:T(8,128)(2,1)} %copy-done.12, bf16[96,2048]{1,0:T(8,128)(2,1)S(1)} %collective-permute-done.9, bf16[96,2048]{1,0:T(8,128)(2,1)S(1)} %collective-permute-done.8), kind=kOutput, calls=%fused_computation | convolution fusion | flops 3227910144 | bytes 11534336 | tf_op jit(solution)/shard_map/dot_general | solution.py:513
  142.3 5.9 %convolution_convert_fusion.1 = bf16[192,2048]{1,0:T(8,128)(2,1)S(1)} fusion(bf16[2048,1024]{1,0:T(8,128)(2,1)} %bitcast.22, bf16[2048,1024]{1,0:T(8,128)(2,1)} %bitcast.19, bf16[96,2048]{1,0:T(8,128)(2,1)} %collective-permute-done.14, bf16[48,2048]{1,0:T(8,128)(2,1)S(1)} %collective-permute-done.13, bf16[48,2048]{1,0:T(8,128)(2,1)S(1)} %collective-permute-done.12), kind=kOutput, calls=%fused_computation.1 | convolution fusion | flops 1613955072 | bytes 9961472 | tf_op jit(solution)/shard_map/dot_general | solution.py:513
  148.4 7.0 %convolution_convert_fusion.2 = bf16[192,2048]{1,0:T(8,128)(2,1)} fusion(bf16[2048,1024]{1,0:T(8,128)(2,1)} %bitcast.23, bf16[2048,1024]{1,0:T(8,128)(2,1)} %bitcast.20, bf16[96,2048]{1,0:T(8,128)(2,1)} %collective-permute-done.6, bf16[96,2048]{1,0:T(8,128)(2,1)} %project.1), kind=kOutput, calls=%fused_computation.2 | convolution fusion | flops 1613168640 | bytes 9961472 | tf_op jit(solution)/shard_map/dot_general | solution.py:513
  158.2 2.0 %collective-permute-start.18 = (bf16[48,2048]{1,0:T(8,128)(2,1)S(1)}, bf16[48,2048]{1,0:T(8,128)(2,1)S(1)}, u32[]{:S(2)}, u32[]{:S(2)}) collective-permute-start(bf16[48,2048]{1,0:T(8,128)(2,1)S(1)} %get-tuple-element.42), channel_id=1, source_target_pairs={{0,2},{2,4},{4,6},{6,0},{1,3},{3,5},{5,7},{7,1},{8,10},{10,12},{12... | collective-permute-start | bytes 589832 | tf_op jit(solution)/shard_map/ppermute | solution.py:304
  160.2 1.4 convert_add_fusion
  161.7 3.4 %collective-permute-done.16 = bf16[48,2048]{1,0:T(8,128)(2,1)S(1)} collective-permute-done((bf16[48,2048]{1,0:T(8,128)(2,1)S(1)}, bf16[48,2048]{1,0:T(8,128)(2,1)S(1)}, u32[]{:S(2)}, u32[]{:S(2)}) %collective-permute-start.16) | collective-permute-done | bytes 196640 | tf_op jit(solution)/shard_map/ppermute | solution.py:304
  167.0 2.9 %collective-permute-start.17 = (bf16[96,2048]{1,0:T(8,128)(2,1)S(1)}, bf16[96,2048]{1,0:T(8,128)(2,1)S(1)}, u32[]{:S(2)}, u32[]{:S(2)}) collective-permute-start(bf16[96,2048]{1,0:T(8,128)(2,1)S(1)} %pad_maximum_fusion.2), channel_id=1, source_target_pairs={{0,6},{2,0},{4,2},{6,4},{1,7},{3,1},{5,3},{7,5},{8,14},{10,8},{12,... | collective-permute-start | bytes 1179656 | tf_op jit(solution)/shard_map/ppermute | solution.py:304
  169.9 8.1 %collective-permute-done.19 = bf16[96,2048]{1,0:T(8,128)(2,1)S(1)} collective-permute-done((bf16[96,2048]{1,0:T(8,128)(2,1)S(1)}, bf16[96,2048]{1,0:T(8,128)(2,1)S(1)}, u32[]{:S(2)}, u32[]{:S(2)}) %collective-permute-start.19) | collective-permute-done | bytes 393248 | tf_op jit(solution)/shard_map/ppermute | solution.py:304
  (79 shorter events, 20.5 us)
Async XLA Ops:
  6.5 120.9 %all-gather.3.cloned.1.call-start = ((), (), s32[]{:S(2)}) async-start(), calls=%async_computation.1 | async-start | bytes 8650752 | tf_op jit(solution)/shard_map/all_gather | solution.py:475
  11.5 63.6 %copy-start.8 = (f32[128]{0:T(128)S(1)}, f32[128]{0:T(128)}, u32[]{:S(2)}) copy-start(f32[128]{0:T(128)} %param.43) | copy-start | bytes 1540
  11.5 63.6 %copy-start.9 = (f32[128]{0:T(128)S(1)}, f32[128]{0:T(128)}, u32[]{:S(2)}) copy-start(f32[128]{0:T(128)} %param.42) | copy-start | bytes 1540
  11.5 63.6 %copy-start.10 = (f32[128]{0:T(128)S(1)}, f32[128]{0:T(128)}, u32[]{:S(2)}) copy-start(f32[128]{0:T(128)} %param.34) | copy-start | bytes 1540
  11.5 63.6 %copy-start.11 = (f32[128]{0:T(128)S(1)}, f32[128]{0:T(128)}, u32[]{:S(2)}) copy-start(f32[128]{0:T(128)} %param.33) | copy-start | bytes 1540
  28.9 6.3 %collective-permute-start = (bf16[384,128]{1,0:T(8,128)(2,1)}, bf16[384,128]{1,0:T(8,128)(2,1)S(1)}, u32[]{:S(2)}, u32[]{:S(2)}) collective-permute-start(bf16[384,128]{1,0:T(8,128)(2,1)} %get-tuple-element.18.own), channel_id=1, source_target_pairs={{0,8},{8,16},{16,24},{24,0},{1,9},{9,17},{17,25},{25,1},{2,10},{10... | collective-permute-start | bytes 294920 | tf_op jit(solution)/shard_map/ppermute | solution.py:304
  30.3 6.8 %collective-permute-start.1 = (bf16[384,128]{1,0:T(8,128)(2,1)}, bf16[384,128]{1,0:T(8,128)(2,1)S(1)}, u32[]{:S(2)}, u32[]{:S(2)}) collective-permute-start(bf16[384,128]{1,0:T(8,128)(2,1)} %get-tuple-element.18.own), channel_id=1, source_target_pairs={{0,16},{8,24},{16,0},{24,8},{1,17},{9,25},{17,1},{25,9},{2,18},{10... | collective-permute-start | bytes 294920 | tf_op jit(solution)/shard_map/ppermute | solution.py:304
  31.1 7.9 %collective-permute-start.2 = (bf16[384,128]{1,0:T(8,128)(2,1)}, bf16[384,128]{1,0:T(8,128)(2,1)S(1)}, u32[]{:S(2)}, u32[]{:S(2)}) collective-permute-start(bf16[384,128]{1,0:T(8,128)(2,1)} %get-tuple-element.18.own), channel_id=1, source_target_pairs={{0,24},{8,0},{16,8},{24,16},{1,25},{9,1},{17,9},{25,17},{2,26},{10... | collective-permute-start | bytes 294920 | tf_op jit(solution)/shard_map/ppermute | solution.py:304
  35.2 3.8 %copy-start.3 = (bf16[384,128]{1,0:T(8,128)(2,1)}, bf16[384,128]{1,0:T(8,128)(2,1)S(1)}, u32[]{:S(2)}) copy-start(bf16[384,128]{1,0:T(8,128)(2,1)S(1)} %collective-permute-done.one) | copy-start | bytes 294916
  37.0 2.0 %copy-start.4 = (bf16[384,128]{1,0:T(8,128)(2,1)}, bf16[384,128]{1,0:T(8,128)(2,1)S(1)}, u32[]{:S(2)}) copy-start(bf16[384,128]{1,0:T(8,128)(2,1)S(1)} %collective-permute-done.1.two) | copy-start | bytes 294916
  42.8 5.7 %collective-permute-start.3 = (bf16[384,128]{1,0:T(8,128)(2,1)S(1)}, bf16[384,128]{1,0:T(8,128)(2,1)S(1)}, u32[]{:S(2)}, u32[]{:S(2)}) collective-permute-start(bf16[384,128]{1,0:T(8,128)(2,1)S(1)} %convert_element_type.65), channel_id=1, source_target_pairs={{0,32},{32,64},{64,96},{96,128},{128,160},{160,192},{192,224},{1,3... | collective-permute-start | bytes 294920 | tf_op jit(solution)/shard_map/ppermute | solution.py:304
  51.9 7.9 %collective-permute-start.4 = (bf16[384,128]{1,0:T(8,128)(2,1)S(1)}, bf16[384,128]{1,0:T(8,128)(2,1)S(1)}, u32[]{:S(2)}, u32[]{:S(2)}) collective-permute-start(bf16[384,128]{1,0:T(8,128)(2,1)S(1)} %convert_element_type.66), channel_id=1, source_target_pairs={{0,64},{32,96},{64,128},{96,160},{128,192},{160,224},{1,65},{33,97... | collective-permute-start | bytes 294920 | tf_op jit(solution)/shard_map/ppermute | solution.py:304
  59.8 0.6 copy-start.6
  63.3 13.5 %collective-permute-start.5 = (bf16[192,128]{1,0:T(8,128)(2,1)S(1)}, bf16[192,128]{1,0:T(8,128)(2,1)S(1)}, u32[]{:S(2)}, u32[]{:S(2)}) collective-permute-start(bf16[192,128]{1,0:T(8,128)(2,1)S(1)} %pad_maximum_fusion.5), channel_id=1, source_target_pairs={{0,128},{32,160},{64,192},{96,224},{1,129},{33,161},{65,193},{97,2... | collective-permute-start | bytes 147464 | tf_op jit(solution)/shard_map/ppermute | solution.py:304
  106.7 10.9 %collective-permute-start.9 = (bf16[96,2048]{1,0:T(8,128)(2,1)}, bf16[96,2048]{1,0:T(8,128)(2,1)S(1)}, u32[]{:S(2)}, u32[]{:S(2)}) collective-permute-start(bf16[96,2048]{1,0:T(8,128)(2,1)} %project.1), channel_id=1, source_target_pairs={{0,6},{2,0},{4,2},{6,4},{1,7},{3,1},{5,3},{7,5},{8,14},{10,8},{12,... | collective-permute-start | bytes 1179656 | tf_op jit(solution)/shard_map/ppermute | solution.py:304
  107.9 12.2 %collective-permute-start.8 = (bf16[96,2048]{1,0:T(8,128)(2,1)}, bf16[96,2048]{1,0:T(8,128)(2,1)S(1)}, u32[]{:S(2)}, u32[]{:S(2)}) collective-permute-start(bf16[96,2048]{1,0:T(8,128)(2,1)} %project.1), channel_id=1, source_target_pairs={{0,2},{2,4},{4,6},{6,0},{1,3},{3,5},{5,7},{7,1},{8,10},{10,12},{12... | collective-permute-start | bytes 1179656 | tf_op jit(solution)/shard_map/ppermute | solution.py:304
  117.6 5.7 %collective-permute-start.13 = (bf16[48,2048]{1,0:T(8,128)(2,1)S(1)}, bf16[48,2048]{1,0:T(8,128)(2,1)S(1)}, u32[]{:S(2)}, u32[]{:S(2)}) collective-permute-start(bf16[48,2048]{1,0:T(8,128)(2,1)S(1)} %slice.95), channel_id=1, source_target_pairs={{0,6},{2,0},{4,2},{6,4},{1,7},{3,1},{5,3},{7,5},{8,14},{10,8},{12,... | collective-permute-start | bytes 589832 | tf_op jit(solution)/shard_map/ppermute | solution.py:304
  120.1 7.0 %collective-permute-start.12 = (bf16[48,2048]{1,0:T(8,128)(2,1)S(1)}, bf16[48,2048]{1,0:T(8,128)(2,1)S(1)}, u32[]{:S(2)}, u32[]{:S(2)}) collective-permute-start(bf16[48,2048]{1,0:T(8,128)(2,1)S(1)} %slice.94), channel_id=1, source_target_pairs={{0,2},{2,4},{4,6},{6,0},{1,3},{3,5},{5,7},{7,1},{8,10},{10,12},{12... | collective-permute-start | bytes 589832 | tf_op jit(solution)/shard_map/ppermute | solution.py:304
  120.3 13.3 %collective-permute-start.10 = (bf16[192,2048]{1,0:T(8,128)(2,1)S(1)}, bf16[192,2048]{1,0:T(8,128)(2,1)S(1)}, u32[]{:S(2)}, u32[]{:S(2)}) collective-permute-start(bf16[192,2048]{1,0:T(8,128)(2,1)S(1)} %pad_maximum_fusion), channel_id=1, source_target_pairs={{0,1},{1,0},{2,3},{3,2},{4,5},{5,4},{6,7},{7,6},{8,9},{9,8},{10,11... | collective-permute-start | bytes 2359304 | tf_op jit(solution)/shard_map/ppermute | solution.py:441
  120.4 28.0 %collective-permute-start.6 = (bf16[96,2048]{1,0:T(8,128)(2,1)}, bf16[96,2048]{1,0:T(8,128)(2,1)}, u32[]{:S(2)}, u32[]{:S(2)}) collective-permute-start(bf16[96,2048]{1,0:T(8,128)(2,1)} %project.1), channel_id=1, source_target_pairs={{0,1},{1,0},{2,3},{3,2},{4,5},{5,4},{6,7},{7,6},{8,9},{9,8},{10,11... | collective-permute-start | bytes 1179656 | tf_op jit(solution)/shard_map/ppermute | solution.py:441
  127.1 15.2 %collective-permute-start.14 = (bf16[96,2048]{1,0:T(8,128)(2,1)S(1)}, bf16[96,2048]{1,0:T(8,128)(2,1)}, u32[]{:S(2)}, u32[]{:S(2)}) collective-permute-start(bf16[96,2048]{1,0:T(8,128)(2,1)S(1)} %pad_maximum_fusion.1), channel_id=1, source_target_pairs={{0,1},{1,0},{2,3},{3,2},{4,5},{5,4},{6,7},{7,6},{8,9},{9,8},{10,11... | collective-permute-start | bytes 1179656 | tf_op jit(solution)/shard_map/ppermute | solution.py:441
  133.6 0.9 copy-start.12
  141.7 18.5 %collective-permute-start.11 = (bf16[192,2048]{1,0:T(8,128)(2,1)S(1)}, bf16[192,2048]{1,0:T(8,128)(2,1)}, u32[]{:S(2)}, u32[]{:S(2)}) collective-permute-start(bf16[192,2048]{1,0:T(8,128)(2,1)S(1)} %slice.91), channel_id=1, source_target_pairs={{0,1},{1,0},{2,3},{3,2},{4,5},{5,4},{6,7},{7,6},{8,9},{9,8},{10,11... | collective-permute-start | bytes 2359304 | tf_op jit(solution)/shard_map/ppermute | solution.py:441
  148.3 8.7 %collective-permute-start.15 = (bf16[96,2048]{1,0:T(8,128)(2,1)S(1)}, bf16[96,2048]{1,0:T(8,128)(2,1)}, u32[]{:S(2)}, u32[]{:S(2)}) collective-permute-start(bf16[96,2048]{1,0:T(8,128)(2,1)S(1)} %slice.97), channel_id=1, source_target_pairs={{0,1},{1,0},{2,3},{3,2},{4,5},{5,4},{6,7},{7,6},{8,9},{9,8},{10,11... | collective-permute-start | bytes 1179656 | tf_op jit(solution)/shard_map/ppermute | solution.py:441
  156.4 13.5 %collective-permute-start.7 = (bf16[96,2048]{1,0:T(8,128)(2,1)S(1)}, bf16[96,2048]{1,0:T(8,128)(2,1)S(1)}, u32[]{:S(2)}, u32[]{:S(2)}) collective-permute-start(bf16[96,2048]{1,0:T(8,128)(2,1)S(1)} %slice.89), channel_id=1, source_target_pairs={{0,1},{1,0},{2,3},{3,2},{4,5},{5,4},{6,7},{7,6},{8,9},{9,8},{10,11... | collective-permute-start | bytes 1179656 | tf_op jit(solution)/shard_map/ppermute | solution.py:441
  158.1 6.9 %collective-permute-start.16 = (bf16[48,2048]{1,0:T(8,128)(2,1)S(1)}, bf16[48,2048]{1,0:T(8,128)(2,1)S(1)}, u32[]{:S(2)}, u32[]{:S(2)}) collective-permute-start(bf16[48,2048]{1,0:T(8,128)(2,1)S(1)} %get-tuple-element.41), channel_id=1, source_target_pairs={{0,6},{2,0},{4,2},{6,4},{1,7},{3,1},{5,3},{7,5},{8,14},{10,8},{12,... | collective-permute-start | bytes 589832 | tf_op jit(solution)/shard_map/ppermute | solution.py:304
  158.2 19.8 %copy-start = (bf16[192,2048]{1,0:T(8,128)(2,1)S(1)}, bf16[192,2048]{1,0:T(8,128)(2,1)}, u32[]{:S(2)}) copy-start(bf16[192,2048]{1,0:T(8,128)(2,1)} %convolution_convert_fusion.2) | copy-start | bytes 2359300
  158.2 19.8 %copy-start.2 = (bf16[96,2048]{1,0:T(8,128)(2,1)S(1)}, bf16[96,2048]{1,0:T(8,128)(2,1)}, u32[]{:S(2)}) copy-start(bf16[96,2048]{1,0:T(8,128)(2,1)} %project.1) | copy-start | bytes 1179652
  158.2 8.1 %collective-permute-start.18 = (bf16[48,2048]{1,0:T(8,128)(2,1)S(1)}, bf16[48,2048]{1,0:T(8,128)(2,1)S(1)}, u32[]{:S(2)}, u32[]{:S(2)}) collective-permute-start(bf16[48,2048]{1,0:T(8,128)(2,1)S(1)} %get-tuple-element.42), channel_id=1, source_target_pairs={{0,2},{2,4},{4,6},{6,0},{1,3},{3,5},{5,7},{7,1},{8,10},{10,12},{12... | collective-permute-start | bytes 589832 | tf_op jit(solution)/shard_map/ppermute | solution.py:304
  166.3 12.3 %copy-start.7 = (f32[2048]{0:T(1024)S(1)}, f32[2048]{0:T(1024)}, u32[]{:S(2)}) copy-start(f32[2048]{0:T(1024)} %param.49) | copy-start | bytes 24580
  166.5 11.5 %collective-permute-start.19 = (bf16[96,2048]{1,0:T(8,128)(2,1)S(1)}, bf16[96,2048]{1,0:T(8,128)(2,1)S(1)}, u32[]{:S(2)}, u32[]{:S(2)}) collective-permute-start(bf16[96,2048]{1,0:T(8,128)(2,1)S(1)} %pad_maximum_fusion.3), channel_id=1, source_target_pairs={{0,2},{2,4},{4,6},{6,0},{1,3},{3,5},{5,7},{7,1},{8,10},{10,12},{12... | collective-permute-start | bytes 1179656 | tf_op jit(solution)/shard_map/ppermute | solution.py:304
  167.0 11.0 %collective-permute-start.17 = (bf16[96,2048]{1,0:T(8,128)(2,1)S(1)}, bf16[96,2048]{1,0:T(8,128)(2,1)S(1)}, u32[]{:S(2)}, u32[]{:S(2)}) collective-permute-start(bf16[96,2048]{1,0:T(8,128)(2,1)S(1)} %pad_maximum_fusion.2), channel_id=1, source_target_pairs={{0,6},{2,0},{4,2},{6,4},{1,7},{3,1},{5,3},{7,5},{8,14},{10,8},{12,... | collective-permute-start | bytes 1179656 | tf_op jit(solution)/shard_map/ppermute | solution.py:304
  (3 other events, 1.9 us)
Sparse Core Ops, SparseCore 0:
  9.9 99.1 all-gather.2
where the time goes:
time: 189 us; the launch traced here: 186 us
  Pallas kernels  39.2 us (21%)
  waiting for transfers between devices  38.9 us (21%)
  starting transfers between devices  37.8 us (20%)
  matrix products  20 us (11%)
  local copies, waits for them, and re-layouts  14.1 us (7%)
  between operations  13.7 us (7%)
  blocking collectives  13.3 us (7%)
  other arithmetic  9.38 us (5%)
    ppermute x14, waiting for transfers between devices, shift(): return lax.ppermute(array, axis, pairs)  38.8 us
    ppermute x14, starting transfers between devices, shift(): return lax.ppermute(array, axis, pairs)  35.7 us
    dot_general x3, matrix products, channel(): lax.dot_general(hidden, down_whole, (((1,), (1,)), ((), ())), preferred_e...  20 us
    pallas_call x1, Pallas kernels, chunk_maps(): pl.pallas_call(maps_kernel, grid=(steps,), in_specs=ins, out_specs=[rows(...  17.4 us
    all_to_all x1, blocking collectives, local(): lax.all_to_all(mixer.reshape(-1, count, 2 * LANES), TP, 0, 0, tiled=True)  13.3 us
    pallas_call x1, Pallas kernels, project(): pl.pallas_call(project_kernel, grid=(peers,), in_specs=[pl.BlockSpec((1,...  8.43 us
    pallas_call x1, Pallas kernels, mixer_outputs(): pl.pallas_call(kernel, grid=(tokens // LANES,), in_specs=[whole(a) for a...  7.49 us
    unnamed x30, local copies, waits for them, and re-layouts  6.72 us
  transfers between devices with their start and end apart: 21, of which 12 were waited for; matrix products, arithmetic and copies ran while one was open for 20% of the time, Pallas kernels for 21%

commit v1 on v0

--- a/solution.py
+++ b/solution.py
@@ -67,21 +67,31 @@
     size = FIRST_HEAD_SIZE if pair else SECOND_HEAD_SIZE
     normed = k * lax.rsqrt(head_mean(k * k, pair) + EPS_KEY) * size ** (-0.5)
     learn = jax.nn.sigmoid(l_ref[...].astype(F32))
-    burst = e_ref[...]
-    if pair:
-        burst = jnp.where(halves(q.shape[0]), burst[:, 0:1], burst[:, 1:2])
+    heads = e_ref.shape[0]
+    rows, cols = iotas(heads, LANES)
+    owner = (cols // size == rows).astype(BF16)
+    burst = sum(mm_tn(part, owner) for part in split3(e_ref[...]))
     logdec = jax.nn.sigmoid(d_ref[...].astype(F32)) * (-(2.718281828459045**-0.5)) + burst
     return q, k, v, normed, learn, logdec
+
+
+def split3(array):
+    high = array.astype(BF16)
+    rest = array - high.astype(F32)
+    mid = rest.astype(BF16)
+    return high, mid, (rest - mid.astype(F32)).astype(BF16)
 
 
 def running_sum(logdec):
     rows, cols = iotas()
     tri = ((rows // CHUNK == cols // CHUNK) & (cols <= rows)).astype(BF16)
-    high = logdec.astype(BF16)
-    rest = logdec - high.astype(F32)
-    mid = rest.astype(BF16)
-    low = (rest - mid.astype(F32)).astype(BF16)
-    return mm(tri, high) + (mm(tri, mid) + mm(tri, low))
+    return jnp.concatenate(
+        [
+            sum(mm(tri, part) for part in split3(logdec[at : at + LANES]))
+            for at in range(0, logdec.shape[0], LANES)
+        ],
+        0,
+    )
 
 
 def chunk_row(array, at):
@@ -110,20 +120,22 @@
 
 def maps_kernel(*refs):
     ins, outs, carry = refs[:12], refs[12:21], refs[21]
+    solved_ref, reads_ref, begin_1, begin_2, starts_q1, starts_z1, starts_q2, starts_z2, total = outs
+    tokens = begin_1.shape[0]
+    blocks, chunks = tokens // LANES, tokens // CHUNK
     step = pl.program_id(0)
     rows, cols = iotas()
     same = rows // CHUNK == cols // CHUNK
     strict = same & (cols < rows)
     inclusive = same & (cols <= rows)
-    eye = (rows == cols).astype(F32)
 
     @pl.when(step == 0)
     def _():
         for g in range(2):
-            carry[g, :LANES, :] = eye
+            carry[g, :LANES, :] = (rows == cols).astype(F32)
             carry[g, LANES:, :] = jnp.zeros((LANES, LANES), F32)
 
-    units = []
+    units = [None] * (3 * blocks)
     keeps = []
     for g in range(2):
         q, k, v, normed, learn, logdec = features(*ins[6 * g : 6 * g + 6], g == 0)
@@ -133,58 +145,54 @@
         middle = chunk_row(cumul, CHUNK // 2)
         ending = chunk_row(cumul, CHUNK - 1)
         up, down, left = jnp.exp(before - middle), jnp.exp(middle - cumul), jnp.exp(ending - cumul)
-        keeps.append([jnp.exp(cumul[c * CHUNK + CHUNK - 1 : (c + 1) * CHUNK]) for c in range(2)])
+        keeps.append(
+            [jnp.exp(cumul[(c + 1) * CHUNK - 1 : (c + 1) * CHUNK]) for c in range(chunks)]
+        )
+        (begin_1, begin_2)[g][...] = (q * jnp.exp(cumul)).astype(BF16)
         parts = (
             forward * up,
             q * jnp.exp(cumul - middle),
             backward * down,
             k * down,
             forward * jnp.exp(before),
-            q * jnp.exp(cumul),
             backward * left,
             k * left,
             v,
         )
-        if g == 0:
-            for c in range(2):
-                units.append([spread(p[c * CHUNK : (c + 1) * CHUNK]) for p in parts])
-        else:
-            units.append(list(parts))
-    units = [[p.astype(BF16) for p in u[:5]] + [u[5]] + [p.astype(BF16) for p in u[6:]] for u in units]
+        for b in range(blocks):
+            if g == 0:
+                for c in range(2):
+                    at = b * LANES + c * CHUNK
+                    units[3 * b + c] = [spread(p[at : at + CHUNK]).astype(BF16) for p in parts]
+            else:
+                units[3 * b + 2] = [p[b * LANES : (b + 1) * LANES].astype(BF16) for p in parts]
     grams = [
         mm_nt(jnp.concatenate([u[0], u[1]], 0), jnp.concatenate([u[2], u[3]], 0)) for u in units
     ]
     lowers = [jnp.where(strict, m[:LANES, :LANES], 0.0) for m in grams]
     writes = [jnp.where(strict, m[:LANES, LANES:], 0.0) for m in grams]
-    read_corr = [jnp.where(inclusive, m[LANES:, :LANES], 0.0) for m in grams]
-    read_write = [jnp.where(inclusive, m[LANES:, LANES:], 0.0) for m in grams]
+    for n, m in enumerate(grams):
+        reads_ref[n, :, :LANES] = jnp.where(inclusive, m[LANES:, :LANES], 0.0).astype(BF16)
+        reads_ref[n, :, LANES:] = jnp.where(inclusive, m[LANES:, LANES:], 0.0).astype(BF16)
     solvers = inverses(lowers)
     sides = [
-        jnp.concatenate([u[4], mm(w, u[8]).astype(BF16)], 1) for u, w in zip(units, writes)
+        jnp.concatenate([u[4], mm(w, u[7]).astype(BF16)], 1) for u, w in zip(units, writes)
     ]
     solved = [mm(x, s).astype(BF16) for x, s in zip(solvers, sides)]
-    carried = [mm(r, s) for r, s in zip(read_corr, solved)]
-    entry = [u[5] + c[:, :LANES] for u, c in zip(units, carried)]
-    inner = [c[:, LANES:] + mm(r, u[8]) for u, c, r in zip(units, carried, read_write)]
-    moved = []
+    moved = [[], []]
     for n, (u, s) in enumerate(zip(units, solved)):
-        for c in range(1 if n < 2 else 2):
-            at = slice(0, LANES) if n < 2 else slice(c * CHUNK, (c + 1) * CHUNK)
-            both = mm_tn(s[at], u[6][at])
-            moved.append((both[:LANES], both[LANES:] + mm_tn(u[8][at], u[7][at])))
-    entry_1, inner_1, entry_2, inner_2, starts_q1, starts_z1, starts_q2, starts_z2, total = outs
-    for c in range(2):
-        at = slice(c * CHUNK, (c + 1) * CHUNK)
-        entry_1[at] = (entry[c][:CHUNK] + entry[c][CHUNK:]).astype(BF16)
-        inner_1[at] = inner[c][:CHUNK] + inner[c][CHUNK:]
-    entry_2[...] = entry[2].astype(BF16)
-    inner_2[...] = inner[2]
+        solved_ref[n] = s
+        g = int(n % 3 == 2)
+        for c in range(1 + g):
+            at = slice(c * CHUNK, (c + 1) * CHUNK) if g else slice(0, LANES)
+            both = mm_tn(s[at], u[5][at])
+            moved[g].append((both[:LANES], both[LANES:] + mm_tn(u[7][at], u[6][at])))
     held = [carry[0], carry[1]]
-    for c in range(2):
+    for c in range(chunks):
         for g, (sq, sz) in enumerate(((starts_q1, starts_z1), (starts_q2, starts_z2))):
             sq[c] = held[g][:LANES].astype(BF16)
             sz[c] = held[g][LANES:]
-            transit, update = moved[2 * g + c]
+            transit, update = moved[g][c]
             after = held[g] * keeps[g][c] + mm(held[g], transit)
             held[g] = jnp.concatenate([after[:LANES], after[LANES:] + update], 0)
     for g in range(2):
@@ -192,32 +200,30 @@
 
     @pl.when(step == pl.num_programs(0) - 1)
     def _():
-        first, second = held
-        total[0:64] = (first[0:64] + first[64:128]).astype(BF16)
-        total[64:128] = (first[128:192] + first[192:256]).astype(BF16)
-        total[128:384] = second.astype(BF16)
+        total[...] = pack(held)
 
 
 def chunk_maps(first, second):
     tokens = first[0].shape[0]
-    steps = tokens // LANES
+    block = 256
     chunks = tokens // CHUNK
-
-    def rows(width=LANES):
-        return pl.BlockSpec((LANES, width), lambda i: (i, 0))
-
-    state = pl.BlockSpec((2, LANES, LANES), lambda i: (i, 0, 0))
+    units = 3 * tokens // LANES
+    rows = pl.BlockSpec((block, LANES), lambda i: (i, 0))
+    state = pl.BlockSpec((block // CHUNK, LANES, LANES), lambda i: (i, 0, 0))
+    unit = pl.BlockSpec((3 * block // LANES, LANES, 2 * LANES), lambda i: (i, 0, 0))
     ins = []
     for group in (first, second):
-        ins += [rows()] * 5 + [rows(group[5].shape[1])]
+        ins += [rows] * 5 + [pl.BlockSpec((group[5].shape[0], block), lambda i: (0, i))]
     return pl.pallas_call(
         maps_kernel,
-        grid=(steps,),
+        grid=(tokens // block,),
         in_specs=ins,
-        out_specs=[rows()] * 4 + [state] * 4 + [pl.BlockSpec((384, LANES), lambda i: (0, 0))],
-        out_shape=[
-            jax.ShapeDtypeStruct((tokens, LANES), t) for t in (BF16, F32, BF16, F32)
-        ]
+        out_specs=[unit] * 2
+        + [rows] * 2
+        + [state] * 4
+        + [pl.BlockSpec((384, LANES), lambda i: (0, 0))],
+        out_shape=[jax.ShapeDtypeStruct((units, LANES, 2 * LANES), BF16)] * 2
+        + [jax.ShapeDtypeStruct((tokens, LANES), BF16)] * 2
         + [jax.ShapeDtypeStruct((chunks, LANES, LANES), t) for t in (BF16, F32, BF16, F32)]
         + [jax.ShapeDtypeStruct((384, LANES), BF16)],
         scratch_shapes=[pltpu.VMEM((2, 2 * LANES, LANES), F32)],
@@ -228,6 +234,43 @@
     )(*first, *second)
 
 
+def reads_kernel(solved, reads, begin_1, begin_2, v_1, v_2, entry_1, inner_1, entry_2, inner_2):
+    for b in range(begin_1.shape[0] // LANES):
+        for u in range(3):
+            n = 3 * b + u
+            at = slice(b * LANES + u * CHUNK, b * LANES + (u + 1) * CHUNK)
+            if u == 2:
+                at = slice(b * LANES, (b + 1) * LANES)
+            value = v_2[at] if u == 2 else spread(v_1[at].astype(F32)).astype(BF16)
+            carried = mm(reads[n, :, :LANES], solved[n])
+            entry = carried[:, :LANES]
+            inner = carried[:, LANES:] + mm(reads[n, :, LANES:], value)
+            if u == 2:
+                entry_2[at] = (begin_2[at].astype(F32) + entry).astype(BF16)
+                inner_2[at] = inner
+            else:
+                entry_1[at] = (begin_1[at].astype(F32) + entry[:CHUNK] + entry[CHUNK:]).astype(BF16)
+                inner_1[at] = inner[:CHUNK] + inner[CHUNK:]
+
+
+def chunk_reads(solved, reads, begin_1, begin_2, v_1, v_2):
+    tokens = begin_1.shape[0]
+    block = 256
+    rows = pl.BlockSpec((block, LANES), lambda i: (i, 0))
+    unit = pl.BlockSpec((3 * block // LANES, LANES, 2 * LANES), lambda i: (i, 0, 0))
+    return pl.pallas_call(
+        reads_kernel,
+        grid=(tokens // block,),
+        in_specs=[unit, unit] + [rows] * 4,
+        out_specs=[rows] * 4,
+        out_shape=[jax.ShapeDtypeStruct((tokens, LANES), t) for t in (BF16, F32, BF16, F32)],
+        cost_estimate=pl.CostEstimate(
+            flops=4_000_000_000, bytes_accessed=6_000_000, transcendentals=0
+        ),
+        name="chunk_reads",
+    )(solved, reads, begin_1, begin_2, v_1, v_2)
+
+
 def unpack(packed):
     def widen(part):
         return spread(part.astype(F32))
@@ -242,7 +285,7 @@
     first, second = pairs
     return jnp.concatenate(
         [first[0:64] + first[64:128], first[128:192] + first[192:256], second], 0
-    )
+    ).astype(BF16)
 
 
 def compose(earlier, later):
@@ -296,7 +339,9 @@
 def join_two_kernel(earlier_ref, before_ref, through_ref, before_out, through_out):
     earlier = unpack(earlier_ref[...])
     before_out[...] = pack(compose(earlier, unpack(before_ref[...])))
-    through_out[...] = pack(compose(earlier, unpack(through_ref[...])))
+    through = pack(compose(earlier, unpack(through_ref[...])))
+    through_out[0:64] = through[64:128]
+    through_out[64:192] = through[256:384]
 
 
 def shift(array, axis, by, size, wrap):
@@ -304,23 +349,24 @@
     return lax.ppermute(array, axis, pairs)
 
 
-def sequence_prefix(total):
-    shape = jax.ShapeDtypeStruct(total.shape, F32)
+def sequence_prefix(total, entries):
+    shape = jax.ShapeDtypeStruct(total.shape, BF16)
     ny, nz = lax.axis_size("y"), lax.axis_size("z")
     peers = [shift(total, "y", s, ny, True) for s in (1, 2, 3)]
+    peers, entries = lax.optimization_barrier((peers, entries))
     mine = lax.axis_index("y").astype(jnp.int32).reshape(1)
     row_before, row_total = vmem_call(
         row_kernel, (shape, shape), mine, total, *peers, scalars=1, name="row_maps"
     )
-    before = shift(row_total.astype(BF16), "z", 1, nz, False)
+    before = shift(row_total, "z", 1, nz, False)
     through = vmem_call(join_kernel, shape, before, row_total, name="join_one")
-    earlier = shift(through.astype(BF16), "z", 2, nz, False)
-    before, through = vmem_call(
-        join_two_kernel, (shape, shape), earlier, before, through, name="join_two"
-    )
-    send = jnp.concatenate([through[64:128], through[256:384]], 0).astype(BF16)
+    earlier = shift(through, "z", 2, nz, False)
+    short = jax.ShapeDtypeStruct((192, LANES), BF16)
+    before, send = vmem_call(
+        join_two_kernel, (shape, short), earlier, before, through, name="join_two"
+    )
     last = shift(send, "z", 4, nz, False)
-    return last, before, row_before
+    return (last, before, row_before), entries
 
 
 def outputs_kernel(*refs):
@@ -341,7 +387,7 @@
         gain, weight = out_params(refs, g)
         start = states[g].astype(BF16)
         pieces = []
-        for c in range(2):
+        for c in range(sq.shape[0]):
             at = slice(c * CHUNK, (c + 1) * CHUNK)
             state = mm(start, sq[c]) + sz[c]
             pieces.append(mm_nt(entry[at], state) + inner[at])
@@ -364,8 +410,9 @@
 
 def mixer_outputs(prefix, groups, params):
     tokens = groups[0][0].shape[0]
-    rows = pl.BlockSpec((LANES, LANES), lambda i: (i, 0))
-    state = pl.BlockSpec((2, LANES, LANES), lambda i: (i, 0, 0))
+    block = 256
+    rows = pl.BlockSpec((block, LANES), lambda i: (i, 0))
+    state = pl.BlockSpec((block // CHUNK, LANES, LANES), lambda i: (i, 0, 0))
 
     def whole(a):
         return pl.BlockSpec(a.shape, lambda i: (0,) * a.ndim)
@@ -376,11 +423,11 @@
 
     return pl.pallas_call(
         kernel,
-        grid=(tokens // LANES,),
+        grid=(tokens // block,),
         in_specs=[whole(a) for a in prefix]
         + [rows, rows, state, state, rows, rows, rows, rows] * 2
         + [whole(params)],
-        out_specs=pl.BlockSpec((LANES, 2 * LANES), lambda i: (i, 0)),
+        out_specs=pl.BlockSpec((block, 2 * LANES), lambda i: (i, 0)),
         out_shape=jax.ShapeDtypeStruct((tokens, 2 * LANES), BF16),
         scratch_shapes=[pltpu.VMEM((2, LANES, LANES), F32)],
         cost_estimate=pl.CostEstimate(
@@ -396,49 +443,108 @@
     return centred * lax.rsqrt(jnp.mean(centred * centred, -1, keepdims=True) + EPS_NORM) * gain
 
 
-def project_kernel(rows_ref, first_ref, second_ref, stream_ref, gain_ref, out_ref, acc):
-    step = pl.program_id(0)
-    rows = rows_ref[0]
-
-    @pl.when(step == 0)
-    def _():
-        acc[...] = ALPHA * stream_ref[...].astype(F32)
-
-    acc[...] += jnp.dot(rows[:, :LANES], first_ref[...], preferred_element_type=F32) + jnp.dot(
-        rows[:, LANES:], second_ref[...], preferred_element_type=F32
-    )
-
-    @pl.when(step == pl.num_programs(0) - 1)
-    def _():
-        out_ref[...] = norm_rows(acc[...], gain_ref[...]).astype(BF16)
+def project_kernel(rows_ref, stream_ref, gain_ref, first, second, out_ref, held, sems):
+    peers = rows_ref.shape[0]
+    copies = []
+    for n in range(peers):
+        at = pl.ds(n * LANES, LANES)
+        for side, source in enumerate((first, second)):
+            copies.append(
+                pltpu.make_async_copy(
+                    source.at[at, :],
+                    held.at[n, pl.ds(side * LANES, LANES), :],
+                    sems.at[n, side],
+                )
+            )
+    for copy in copies:
+        copy.start()
+    total = ALPHA * stream_ref[...].astype(F32)
+    for n in range(peers):
+        copies[2 * n].wait()
+        copies[2 * n + 1].wait()
+        total += jnp.dot(rows_ref[n], held[n], preferred_element_type=F32)
+    out_ref[...] = norm_rows(total, gain_ref[...]).astype(BF16)
 
 
 def project(rows, first, second, stream, gain):
     peers, count, _ = rows.shape
     width = first.shape[1]
-    weight = pl.BlockSpec((LANES, width), lambda i: (i, 0))
+    near = pl.BlockSpec(memory_space=pltpu.VMEM)
+    far = pl.BlockSpec(memory_space=pl.ANY)
     return pl.pallas_call(
         project_kernel,
-        grid=(peers,),
-        in_specs=[
-            pl.BlockSpec((1, count, 2 * LANES), lambda i: (i, 0, 0)),
-            weight,
-            weight,
-            pl.BlockSpec((count, width), lambda i: (0, 0)),
-            pl.BlockSpec((1, width), lambda i: (0, 0)),
+        in_specs=[near, near, near, far, far],
+        out_specs=near,
+        out_shape=jax.ShapeDtypeStruct((count, width), BF16),
+        scratch_shapes=[
+            pltpu.VMEM((peers, 2 * LANES, width), BF16),
+            pltpu.SemaphoreType.DMA((peers, 2)),
         ],
-        out_specs=pl.BlockSpec((count, width), lambda i: (0, 0)),
-        out_shape=jax.ShapeDtypeStruct((count, width), BF16),
-        scratch_shapes=[pltpu.VMEM((count, width), F32)],
         cost_estimate=pl.CostEstimate(
             flops=4_000_000_000, bytes_accessed=9_000_000, transcendentals=100
         ),
         name="project",
-    )(rows, first, second, stream, gain.reshape(1, -1))
+    )(rows, stream, gain.reshape(1, -1), first, second)
 
 
 def swap_core(array):
     return lax.ppermute(array, "c", [(0, 1), (1, 0)])
+
+
+def channel_kernel(mine_ref, theirs_ref, weights, mine_out, theirs_out, rows, acc, held, sems):
+    count, width = mine_ref.shape
+    pieces, group, depth, _ = held.shape
+    half = pieces // 2
+    block = group * depth
+    copies = []
+    for n in range(pieces):
+        side = weights.at[
+            pl.ds((n % half) * group, group), pl.ds((n // half) * depth, depth), :
+        ]
+        copies.append(pltpu.make_async_copy(side, held.at[n], sems.at[n]))
+    for copy in copies:
+        copy.start()
+    for n in range(half):
+        at = slice(n * block, (n + 1) * block)
+        rows[n, :count] = mine_ref[:, at]
+        rows[n, count:] = theirs_ref[:, at]
+    for n in range(half):
+        copies[n].wait()
+        part = jnp.dot(rows[n], held[n].reshape(block, -1), preferred_element_type=F32)
+        acc[...] = part if n == 0 else acc[...] + part
+    hidden = jnp.square(jnp.maximum(acc[...], 0.0)).astype(BF16)
+    for n in range(half):
+        copies[half + n].wait()
+        part = mm_nt(hidden, held[half + n].reshape(block, -1)).astype(BF16)
+        at = slice(n * block, (n + 1) * block)
+        mine_out[:, at] = part[:count]
+        theirs_out[:, at] = part[count:]
+
+
+def channel(mine, theirs, weights):
+    count, width = mine.shape
+    peers, depth, hidden = weights.shape
+    pieces = 8
+    group = 2 * peers // pieces
+    rows = pl.BlockSpec(memory_space=pltpu.VMEM)
+    return pl.pallas_call(
+        channel_kernel,
+        in_specs=[rows, rows, pl.BlockSpec(memory_space=pl.ANY)],
+        out_specs=[rows, rows],
+        out_shape=[jax.ShapeDtypeStruct((count, width), BF16)] * 2,
+        scratch_shapes=[
+            pltpu.VMEM((pieces // 2, 2 * count, 2 * width // pieces), BF16),
+            pltpu.VMEM((2 * count, hidden), F32),
+            pltpu.VMEM((pieces, group, depth // 2, hidden), BF16),
+            pltpu.SemaphoreType.DMA((pieces,)),
+        ],
+        cost_estimate=pl.CostEstimate(
+            flops=8 * count * width * hidden,
+            bytes_accessed=2 * peers * depth * hidden,
+            transcendentals=0,
+        ),
+        name="channel",
+    )(mine, theirs, weights)
 
 
 def local(
@@ -469,19 +575,22 @@
     final_norm_gain,
 ):
     count, width = stream.shape
-    depth = mixer_up_weight.shape[0]
-    hidden_width = mixer_up_weight.shape[1]
     both = jnp.concatenate([mixer_up_weight, mixer_down_weight.T], 0)
     weights = lax.all_gather(both, SP)
-    up_whole = weights[:, :depth].reshape(-1, hidden_width)
-    down_whole = weights[:, depth:].reshape(-1, hidden_width)
-
-    maps = chunk_maps(
-        (query_first, key_first, value_first, decay_first, learning_first, extra_decay_first),
-        (query_second, key_second, value_second, decay_second, learning_second, extra_decay_second),
-    )
-    entry_1, inner_1, entry_2, inner_2, sq1, sz1, sq2, sz2, total = maps
-    prefix = sequence_prefix(total)
+
+    solved, reads, begin_1, begin_2, sq1, sz1, sq2, sz2, total = chunk_maps(
+        (query_first, key_first, value_first, decay_first, learning_first, extra_decay_first.T),
+        (
+            query_second,
+            key_second,
+            value_second,
+            decay_second,
+            learning_second,
+            extra_decay_second.T,
+        ),
+    )
+    entries = chunk_reads(solved, reads, begin_1, begin_2, value_first, value_second)
+    prefix, (entry_1, inner_1, entry_2, inner_2) = sequence_prefix(total, entries)
     params = jnp.stack(
         [head_norm_gain_first, self_weight_first, head_norm_gain_second, self_weight_second]
     )
@@ -502,32 +611,38 @@
     half = count // 2
     near_p = shift(middle, "x", 1, nx, True)
     near_m = shift(middle, "x", -1, nx, True)
-    far_p = shift(near_p[:half], "x", 1, nx, True)
-    far_m = shift(near_m[half:], "x", -1, nx, True)
-    far = jnp.concatenate([far_p, far_m], 0)
-
-    def channel(block):
-        rows_all = jnp.concatenate([block, swap_core(block)], 0)
-        upward = jnp.dot(rows_all, up_whole, preferred_element_type=F32)
-        hidden = jnp.square(jax.nn.relu(upward)).astype(BF16)
-        part = lax.dot_general(
-            hidden, down_whole, (((1,), (1,)), ((), ())), preferred_element_type=F32
-        ).astype(BF16)
-        size = block.shape[0]
-        return part[:size].astype(F32) + swap_core(part[size:]).astype(F32)
-
-    sum_own = channel(middle)
-    sum_near = channel(jnp.concatenate([near_p, near_m], 0))
-    sum_far = channel(far)
-    sum_p, sum_m = sum_near[:count], sum_near[count:]
-    from_p = shift(sum_far[:half].astype(BF16), "x", 1, nx, True).astype(F32)
-    from_m = shift(sum_far[half:].astype(BF16), "x", -1, nx, True).astype(F32)
-    sum_m = jnp.concatenate([sum_m[:half] + from_p, sum_m[half:]], 0).astype(BF16)
-    sum_p = jnp.concatenate([sum_p[:half], sum_p[half:] + from_m], 0).astype(BF16)
+    far = jnp.concatenate(
+        [shift(near_p[:half], "x", 1, nx, True), shift(near_m[half:], "x", -1, nx, True)], 0
+    )
+    near = jnp.concatenate([near_p, near_m], 0)
+    own_there = swap_core(middle)
+    near_there = swap_core(near)
+    far_there = swap_core(far)
+
+    far_part, far_send = channel(far, far_there, weights)
+    far_back = swap_core(far_send)
+    near_part, near_send = channel(near, near_there, weights)
+    near_back = swap_core(near_send)
+    own_part, own_send = channel(middle, own_there, weights)
+    own_back = swap_core(own_send)
+
+    def total_of(part, back, at, more=None):
+        out = part[at : at + half].astype(F32) + back[at : at + half].astype(F32)
+        if more is not None:
+            out = out + more.astype(F32)
+        return out.astype(BF16)
+
+    from_p = shift(total_of(far_part, far_back, 0), "x", 1, nx, True)
+    from_m = shift(total_of(far_part, far_back, half), "x", -1, nx, True)
+    back_p_first = shift(total_of(near_part, near_back, 0), "x", -1, nx, True)
+    back_m_second = shift(total_of(near_part, near_back, 3 * half), "x", 1, nx, True)
+    back_p_second = shift(total_of(near_part, near_back, half, from_m), "x", -1, nx, True)
+    back_m_first = shift(total_of(near_part, near_back, 2 * half, from_p), "x", 1, nx, True)
     ff_total = (
-        sum_own
-        + shift(sum_p, "x", -1, nx, True).astype(F32)
-        + shift(sum_m, "x", 1, nx, True).astype(F32)
+        own_part.astype(F32)
+        + own_back.astype(F32)
+        + jnp.concatenate([back_p_first, back_p_second], 0).astype(F32)
+        + jnp.concatenate([back_m_first, back_m_second], 0).astype(F32)
     )
     return norm_rows(ALPHA * middle.astype(F32) + ff_total, final_norm_gain).astype(BF16)
 

time: 189 us -> 172 us (0.910)
  matrix products: 20 us -> 0 us
  Pallas kernels: 39.2 us -> 55.6 us
  local copies, waits for them, and re-layouts: 14.1 us -> 5.06 us
  starting transfers between devices: 37.8 us -> 43.4 us
  waiting for transfers between devices: 38.9 us -> 34.8 us
  other arithmetic: 9.38 us -> 5.36 us
    dot_general x3 -> x0, matrix products: 20 us -> none  [channel(): lax.dot_general(hidden, down_whole, (((1,), (1,)), ((), ())), preferred_e...]
    pallas_call x3 -> x7, Pallas kernels: 33.3 us -> 49.9 us  [the longest x3 21.4 us: channel(): pl.pallas_call(channel_kernel, in_specs=[rows, rows, pl.BlockSpec(memory_...]
    slice x10 -> x2, local copies, waits for them, and re-layouts: 7.41 us -> 0.03 us  [the longest x1 0.01 us: local(): near_m[half:]]
    ppermute x14 -> x16, starting transfers between devices: 35.7 us -> 42 us  [shift(): return lax.ppermute(array, axis, pairs)]
    ppermute x14 -> x16, waiting for transfers between devices: 38.8 us -> 33.1 us  [shift(): return lax.ppermute(array, axis, pairs)]
    another operation x3 -> x0, other arithmetic: 2.1 us -> none
    unnamed x30 -> x38, local copies, waits for them, and re-layouts: 6.72 us -> 4.99 us
  transfers between devices with their start and end apart: 21 -> 23, of which waited for: 12 -> 12; matrix products, arithmetic and copies ran while one was open for 20% -> 1% of each run, Pallas kernels for 21% -> 32%
where the time goes in v1:
time: 172 us; the launch traced here: 171 us
  Pallas kernels  55.6 us (32%)
  starting transfers between devices  43.4 us (25%)
  waiting for transfers between devices  34.8 us (20%)
  between operations  13.7 us (8%)
  blocking collectives  13.3 us (8%)
  other arithmetic  5.36 us (3%)
  local copies, waits for them, and re-layouts  5.06 us (3%)
    ppermute x16, starting transfers between devices, shift(): return lax.ppermute(array, axis, pairs)  42 us
    ppermute x16, waiting for transfers between devices, shift(): return lax.ppermute(array, axis, pairs)  33.1 us
    pallas_call x3, Pallas kernels, channel(): pl.pallas_call(channel_kernel, in_specs=[rows, rows, pl.BlockSpec(memory_...  21.4 us
    all_to_all x1, blocking collectives, local(): lax.all_to_all(mixer.reshape(-1, count, 2 * LANES), TP, 0, 0, tiled=True)  13.3 us
    pallas_call x1, Pallas kernels, chunk_maps(): pl.pallas_call(maps_kernel, grid=(tokens // block,), in_specs=ins, out_sp...  12.2 us
    pallas_call x1, Pallas kernels, mixer_outputs(): pl.pallas_call(kernel, grid=(tokens // block,), in_specs=[whole(a) for a...  6.13 us
    pallas_call x1, Pallas kernels, project(): pl.pallas_call(project_kernel, in_specs=[near, near, near, far, far], out...  6.09 us
    pallas_call x3, Pallas kernels, vmem_call(): pl.pallas_call(kernel, in_specs=[pl.BlockSpec(memory_space=pltpu.SMEM)] *...  5.71 us
  transfers between devices with their start and end apart: 23, of which 12 were waited for; matrix products, arithmetic and copies ran while one was open for 1% of the time, Pallas kernels for 32%

profile of v1, /device:TPU:16, one launch (start us, length us, event | category | flops | bytes accessed | tf_op | source)
XLA Modules:
  0.0 171.2 jit_solution(10448699033379116863)
XLA Ops:
  6.5 1.7 pad_maximum_fusion
  8.2 12.2 %chunk_maps.1 = (bf16[18,128,256]{2,1,0:T(8,128)(2,1)}, bf16[18,128,256]{2,1,0:T(8,128)(2,1)}, bf16[768,128]{1,0:T(8,128)(2,1)}, bf16[768,128]{1,0:T(8,128)(2,1)...) custom-call(bf16[768,128]{1,0:T(8,128)(2,1)} %refs_7_.3, ...), custom_call_target="tpu_custom_call" | custom-call | flops 12000000000 | bytes 8000000 | tf_op jit(solution)/shard_map/chunk_maps/pallas_call | solution.py:217
  22.7 2.5 %collective-permute-start.2 = (bf16[384,128]{1,0:T(8,128)(2,1)}, bf16[384,128]{1,0:T(8,128)(2,1)S(1)}, u32[]{:S(2)}, u32[]{:S(2)}) collective-permute-start(bf16[384,128]{1,0:T(8,128)(2,1)} %get-tuple-element.35.own), channel_id=1, source_target_pairs={{0,24},{8,0},{16,8},{24,16},{1,25},{9,1},{17,9},{25,17},{2,26},{10... | collective-permute-start | bytes 294920 | tf_op jit(solution)/shard_map/ppermute | solution.py:349
  25.2 4.0 %chunk_reads.1 = (bf16[768,128]{1,0:T(8,128)(2,1)}, f32[768,128]{1,0:T(8,128)}, bf16[768,128]{1,0:T(8,128)(2,1)}, f32[768,128]{1,0:T(8,128)}) custom-call(bf16[18,128,256]{2,1,0:T(8,128)(2,1)} %get-tuple-element.36.solved, bf16[18,128,256]{2,1,0:T(8,128)(2,1)} %get-tuple-element.37.reads, bf16[768,128]{1,0:T(8,128)(2,1)} %get-tuple-element.38.begin_1, ...), custom_call_target="tpu_custom_call" | custom-call | flops 4000000000 | bytes 6000000 | tf_op jit(solution)/shard_map/chunk_reads/pallas_call | solution.py:261
  29.2 1.5 collective-permute-done.2.three
  31.4 2.1 %row_maps.1 = (bf16[384,128]{1,0:T(8,128)(2,1)}, bf16[384,128]{1,0:T(8,128)(2,1)}) custom-call(s32[1]{0:T(128)} %bitcast.mine_ref, bf16[384,128]{1,0:T(8,128)(2,1)} %get-tuple-element.35.own, bf16[384,128]{1,0:T(8,128)(2,1)} %copy-done.7, bf16[384,128]{1,0:T(8,128)(2,1)} %copy-done.8, bf16[384,128]{1,0:T(8,128)(2,1)} %copy-done.9), custom_call_target="tpu_custom_call" | custom-call | tf_op jit(solution)/shard_map/row_maps/pallas_call | solution.py:325
  33.6 4.0 %collective-permute-start.3 = (bf16[384,128]{1,0:T(8,128)(2,1)}, bf16[384,128]{1,0:T(8,128)(2,1)S(1)}, u32[]{:S(2)}, u32[]{:S(2)}) collective-permute-start(bf16[384,128]{1,0:T(8,128)(2,1)} %get-tuple-element.47.later_ref), channel_id=1, source_target_pairs={{0,32},{32,64},{64,96},{96,128},{128,160},{160,192},{192,224},{1,3... | collective-permute-start | bytes 294920 | tf_op jit(solution)/shard_map/ppermute | solution.py:349
  37.6 3.3 %collective-permute-done.3.earlier_ref.before_ref = bf16[384,128]{1,0:T(8,128)(2,1)S(1)} collective-permute-done((bf16[384,128]{1,0:T(8,128)(2,1)}, bf16[384,128]{1,0:T(8,128)(2,1)S(1)}, u32[]{:S(2)}, u32[]{:S(2)}) %collective-permute-start.3) | collective-permute-done | bytes 98336 | tf_op jit(solution)/shard_map/ppermute | solution.py:349
  41.5 1.7 %join_one.1.through_ref = bf16[384,128]{1,0:T(8,128)(2,1)} custom-call(bf16[384,128]{1,0:T(8,128)(2,1)} %copy-done.5, bf16[384,128]{1,0:T(8,128)(2,1)} %get-tuple-element.47.later_ref), custom_call_target="tpu_custom_call" | custom-call | tf_op jit(solution)/shard_map/join_one/pallas_call | solution.py:325
  43.3 5.4 %collective-permute-start.4 = (bf16[384,128]{1,0:T(8,128)(2,1)}, bf16[384,128]{1,0:T(8,128)(2,1)S(1)}, u32[]{:S(2)}, u32[]{:S(2)}) collective-permute-start(bf16[384,128]{1,0:T(8,128)(2,1)} %join_one.1.through_ref), channel_id=1, source_target_pairs={{0,64},{32,96},{64,128},{96,160},{128,192},{160,224},{1,65},{33,97... | collective-permute-start | bytes 294920 | tf_op jit(solution)/shard_map/ppermute | solution.py:349
  48.7 2.8 %collective-permute-done.4.earlier_ref = bf16[384,128]{1,0:T(8,128)(2,1)S(1)} collective-permute-done((bf16[384,128]{1,0:T(8,128)(2,1)}, bf16[384,128]{1,0:T(8,128)(2,1)S(1)}, u32[]{:S(2)}, u32[]{:S(2)}) %collective-permute-start.4) | collective-permute-done | bytes 98336 | tf_op jit(solution)/shard_map/ppermute | solution.py:349
  52.1 1.8 %join_two.1 = (bf16[384,128]{1,0:T(8,128)(2,1)}, bf16[192,128]{1,0:T(8,128)(2,1)}) custom-call(bf16[384,128]{1,0:T(8,128)(2,1)} %copy-done.10, bf16[384,128]{1,0:T(8,128)(2,1)} %copy-done.5, bf16[384,128]{1,0:T(8,128)(2,1)} %join_one.1.through_ref), custom_call_target="tpu_custom_call" | custom-call | tf_op jit(solution)/shard_map/join_two/pallas_call | solution.py:325
  53.9 12.7 %collective-permute-start.5 = (bf16[192,128]{1,0:T(8,128)(2,1)}, bf16[192,128]{1,0:T(8,128)(2,1)S(1)}, u32[]{:S(2)}, u32[]{:S(2)}) collective-permute-start(bf16[192,128]{1,0:T(8,128)(2,1)} %get-tuple-element.48), channel_id=1, source_target_pairs={{0,128},{32,160},{64,192},{96,224},{1,129},{33,161},{65,193},{97,2... | collective-permute-start | bytes 147464 | tf_op jit(solution)/shard_map/ppermute | solution.py:349
  67.3 2.5 %collective-permute-done.5.refs_0_ = bf16[192,128]{1,0:T(8,128)(2,1)S(1)} collective-permute-done((bf16[192,128]{1,0:T(8,128)(2,1)}, bf16[192,128]{1,0:T(8,128)(2,1)S(1)}, u32[]{:S(2)}, u32[]{:S(2)}) %collective-permute-start.5) | collective-permute-done | bytes 49184 | tf_op jit(solution)/shard_map/ppermute | solution.py:349
  70.4 6.1 %mixer_outputs.1 = bf16[768,256]{1,0:T(8,128)(2,1)} custom-call(bf16[192,128]{1,0:T(8,128)(2,1)} %copy-done.17, bf16[384,128]{1,0:T(8,128)(2,1)} %get-tuple-element.49.refs_1_, bf16[384,128]{1,0:T(8,128)(2,1)} %get-tuple-element.50.refs_2_, bf16[768,128]{1,0:T(8,128)(2,1)} %get-tuple-element.51.refs_3_, f32[768,128]{1,0:T(8,128)} %get-tuple-element.52.refs_4_, ...), custom_call_target="tpu_custom_call" | custom-call | flops 2000000000 | bytes 6000000 | tf_op jit(solution)/shard_map/mixer_outputs/pallas_call | solution.py:424
  76.5 13.3 %all_to_all.5.rows_ref = bf16[8,96,256]{2,1,0:T(8,128)(2,1)} all-to-all(bf16[8,96,256]{2,1,0:T(8,128)(2,1)} %bitcast.14), channel_id=1, replica_groups=mesh['z'=8,'y'=4,'x'=4,'c'=2] {'x','c'}, dimensions={0} | all-to-all | bytes 786432 | tf_op jit(solution)/shard_map/all_to_all | solution.py:605
  89.8 6.1 %project.1.mine_ref = bf16[96,2048]{1,0:T(8,128)(2,1)} custom-call(bf16[8,96,256]{2,1,0:T(8,128)(2,1)} %all_to_all.5.rows_ref, bf16[96,2048]{1,0:T(8,128)(2,1)} %stream_ref.1, f32[1,2048]{1,0:T(1,128)} %bitcast.20, bf16[1024,2048]{1,0:T(8,128)(2,1)} %first.1, bf16[1024,2048]{1,0:T(8,128)(2,1)} %second.1), custom_call_target="tpu_custom_call" | custom-call | flops 4000000000 | bytes 9000000 | tf_op jit(solution)/shard_map/project/pallas_call | solution.py:474
  96.5 2.7 %collective-permute-start.9 = (bf16[96,2048]{1,0:T(8,128)(2,1)}, bf16[96,2048]{1,0:T(8,128)(2,1)S(1)}, u32[]{:S(2)}, u32[]{:S(2)}) collective-permute-start(bf16[96,2048]{1,0:T(8,128)(2,1)} %project.1.mine_ref), channel_id=1, source_target_pairs={{0,6},{2,0},{4,2},{6,4},{1,7},{3,1},{5,3},{7,5},{8,14},{10,8},{12,... | collective-permute-start | bytes 1179656 | tf_op jit(solution)/shard_map/ppermute | solution.py:349
  99.2 8.8 %collective-permute-done.8 = bf16[96,2048]{1,0:T(8,128)(2,1)S(1)} collective-permute-done((bf16[96,2048]{1,0:T(8,128)(2,1)}, bf16[96,2048]{1,0:T(8,128)(2,1)S(1)}, u32[]{:S(2)}, u32[]{:S(2)}) %collective-permute-start.8) | collective-permute-done | bytes 393248 | tf_op jit(solution)/shard_map/ppermute | solution.py:349
  108.2 3.3 %collective-permute-start.14 = (bf16[48,2048]{1,0:T(8,128)(2,1)S(1)}, bf16[48,2048]{1,0:T(8,128)(2,1)S(1)}, u32[]{:S(2)}, u32[]{:S(2)}) collective-permute-start(bf16[48,2048]{1,0:T(8,128)(2,1)S(1)} %slice.59), channel_id=1, source_target_pairs={{0,6},{2,0},{4,2},{6,4},{1,7},{3,1},{5,3},{7,5},{8,14},{10,8},{12,... | collective-permute-start | bytes 589832 | tf_op jit(solution)/shard_map/ppermute | solution.py:349
  111.8 3.2 %collective-permute-done.13 = bf16[48,2048]{1,0:T(8,128)(2,1)S(1)} collective-permute-done((bf16[48,2048]{1,0:T(8,128)(2,1)S(1)}, bf16[48,2048]{1,0:T(8,128)(2,1)S(1)}, u32[]{:S(2)}, u32[]{:S(2)}) %collective-permute-start.13) | collective-permute-done | bytes 196640 | tf_op jit(solution)/shard_map/ppermute | solution.py:349
  115.2 1.7 collective-permute-done.15.theirs_ref
  117.6 6.6 %channel.5 = (bf16[96,2048]{1,0:T(8,128)(2,1)}, bf16[96,2048]{1,0:T(8,128)(2,1)}) custom-call(bf16[96,2048]{1,0:T(8,128)(2,1)} %copy-done, bf16[96,2048]{1,0:T(8,128)(2,1)} %copy-done.3, bf16[32,128,1024]{2,1,0:T(8,128)(2,1)} %bitcast.11), custom_call_target="tpu_custom_call" | custom-call | flops 1610612736 | bytes 8388608 | tf_op jit(solution)/shard_map/channel/pallas_call | solution.py:530
  125.4 8.1 %channel.4 = (bf16[192,2048]{1,0:T(8,128)(2,1)}, bf16[192,2048]{1,0:T(8,128)(2,1)}) custom-call(bf16[192,2048]{1,0:T(8,128)(2,1)} %copy-done.6, bf16[192,2048]{1,0:T(8,128)(2,1)} %copy-done.16, bf16[32,128,1024]{2,1,0:T(8,128)(2,1)} %bitcast.12), custom_call_target="tpu_custom_call" | custom-call | flops 3221225472 | bytes 8388608 | tf_op jit(solution)/shard_map/channel/pallas_call | solution.py:530
  134.3 3.4 %collective-permute-start.17 = (bf16[48,2048]{1,0:T(8,128)(2,1)S(1)}, bf16[48,2048]{1,0:T(8,128)(2,1)S(1)}, u32[]{:S(2)}, u32[]{:S(2)}) collective-permute-start(bf16[48,2048]{1,0:T(8,128)(2,1)S(1)} %get-tuple-element.71), channel_id=1, source_target_pairs={{0,6},{2,0},{4,2},{6,4},{1,7},{3,1},{5,3},{7,5},{8,14},{10,8},{12,... | collective-permute-start | bytes 589832 | tf_op jit(solution)/shard_map/ppermute | solution.py:349
  138.4 6.6 %channel.3 = (bf16[96,2048]{1,0:T(8,128)(2,1)}, bf16[96,2048]{1,0:T(8,128)(2,1)}) custom-call(bf16[96,2048]{1,0:T(8,128)(2,1)} %project.1.mine_ref, bf16[96,2048]{1,0:T(8,128)(2,1)} %copy-done.2, bf16[32,128,1024]{2,1,0:T(8,128)(2,1)} %bitcast.13), custom_call_target="tpu_custom_call" | custom-call | flops 1610612736 | bytes 8388608 | tf_op jit(solution)/shard_map/channel/pallas_call | solution.py:530
  146.1 3.0 %collective-permute-start.12 = (bf16[48,2048]{1,0:T(8,128)(2,1)S(1)}, bf16[48,2048]{1,0:T(8,128)(2,1)S(1)}, u32[]{:S(2)}, u32[]{:S(2)}) collective-permute-start(bf16[48,2048]{1,0:T(8,128)(2,1)S(1)} %get-tuple-element.67), channel_id=1, source_target_pairs={{0,6},{2,0},{4,2},{6,4},{1,7},{3,1},{5,3},{7,5},{8,14},{10,8},{12,... | collective-permute-start | bytes 589832 | tf_op jit(solution)/shard_map/ppermute | solution.py:349
  149.2 1.9 %collective-permute-start.20 = (bf16[48,2048]{1,0:T(8,128)(2,1)S(1)}, bf16[48,2048]{1,0:T(8,128)(2,1)S(1)}, u32[]{:S(2)}, u32[]{:S(2)}) collective-permute-start(bf16[48,2048]{1,0:T(8,128)(2,1)S(1)} %get-tuple-element.69), channel_id=1, source_target_pairs={{0,2},{2,4},{4,6},{6,0},{1,3},{3,5},{5,7},{7,1},{8,10},{10,12},{12... | collective-permute-start | bytes 589832 | tf_op jit(solution)/shard_map/ppermute | solution.py:349
  151.1 3.2 %collective-permute-done.12 = bf16[48,2048]{1,0:T(8,128)(2,1)S(1)} collective-permute-done((bf16[48,2048]{1,0:T(8,128)(2,1)S(1)}, bf16[48,2048]{1,0:T(8,128)(2,1)S(1)}, u32[]{:S(2)}, u32[]{:S(2)}) %collective-permute-start.12) | collective-permute-done | bytes 196640 | tf_op jit(solution)/shard_map/ppermute | solution.py:349
  154.4 3.7 %collective-permute-done.18 = bf16[48,2048]{1,0:T(8,128)(2,1)S(1)} collective-permute-done((bf16[48,2048]{1,0:T(8,128)(2,1)S(1)}, bf16[48,2048]{1,0:T(8,128)(2,1)S(1)}, u32[]{:S(2)}, u32[]{:S(2)}) %collective-permute-start.18) | collective-permute-done | bytes 196640 | tf_op jit(solution)/shard_map/ppermute | solution.py:349
  158.2 3.4 %collective-permute-done.21 = bf16[48,2048]{1,0:T(8,128)(2,1)S(1)} collective-permute-done((bf16[48,2048]{1,0:T(8,128)(2,1)S(1)}, bf16[48,2048]{1,0:T(8,128)(2,1)S(1)}, u32[]{:S(2)}, u32[]{:S(2)}) %collective-permute-start.21) | collective-permute-done | bytes 196640 | tf_op jit(solution)/shard_map/ppermute | solution.py:349
  161.6 1.5 fusion
  (77 shorter events, 12.3 us)
Async XLA Ops:
  6.5 110.3 %all-gather.3.cloned.1.call-start = ((), (), s32[]{:S(2)}) async-start(), calls=%async_computation.1 | async-start | bytes 8650752 | tf_op jit(solution)/shard_map/all_gather | solution.py:579
  20.4 8.8 %collective-permute-start = (bf16[384,128]{1,0:T(8,128)(2,1)}, bf16[384,128]{1,0:T(8,128)(2,1)S(1)}, u32[]{:S(2)}, u32[]{:S(2)}) collective-permute-start(bf16[384,128]{1,0:T(8,128)(2,1)} %get-tuple-element.35.own), channel_id=1, source_target_pairs={{0,8},{8,16},{16,24},{24,0},{1,9},{9,17},{17,25},{25,1},{2,10},{10... | collective-permute-start | bytes 294920 | tf_op jit(solution)/shard_map/ppermute | solution.py:349
  21.8 7.4 %collective-permute-start.1 = (bf16[384,128]{1,0:T(8,128)(2,1)}, bf16[384,128]{1,0:T(8,128)(2,1)S(1)}, u32[]{:S(2)}, u32[]{:S(2)}) collective-permute-start(bf16[384,128]{1,0:T(8,128)(2,1)} %get-tuple-element.35.own), channel_id=1, source_target_pairs={{0,16},{8,24},{16,0},{24,8},{1,17},{9,25},{17,1},{25,9},{2,18},{10... | collective-permute-start | bytes 294920 | tf_op jit(solution)/shard_map/ppermute | solution.py:349
  22.7 8.1 %collective-permute-start.2 = (bf16[384,128]{1,0:T(8,128)(2,1)}, bf16[384,128]{1,0:T(8,128)(2,1)S(1)}, u32[]{:S(2)}, u32[]{:S(2)}) collective-permute-start(bf16[384,128]{1,0:T(8,128)(2,1)} %get-tuple-element.35.own), channel_id=1, source_target_pairs={{0,24},{8,0},{16,8},{24,16},{1,25},{9,1},{17,9},{25,17},{2,26},{10... | collective-permute-start | bytes 294920 | tf_op jit(solution)/shard_map/ppermute | solution.py:349
  25.2 41.5 %copy-start.12 = (f32[128]{0:T(128)S(1)}, f32[128]{0:T(128)}, u32[]{:S(2)}) copy-start(f32[128]{0:T(128)} %param.43) | copy-start | bytes 1540
  25.2 41.5 %copy-start.13 = (f32[128]{0:T(128)S(1)}, f32[128]{0:T(128)}, u32[]{:S(2)}) copy-start(f32[128]{0:T(128)} %param.42) | copy-start | bytes 1540
  25.2 41.5 %copy-start.14 = (f32[128]{0:T(128)S(1)}, f32[128]{0:T(128)}, u32[]{:S(2)}) copy-start(f32[128]{0:T(128)} %param.34) | copy-start | bytes 1540
  25.2 41.5 %copy-start.15 = (f32[128]{0:T(128)S(1)}, f32[128]{0:T(128)}, u32[]{:S(2)}) copy-start(f32[128]{0:T(128)} %param.33) | copy-start | bytes 1540
  33.6 7.3 %collective-permute-start.3 = (bf16[384,128]{1,0:T(8,128)(2,1)}, bf16[384,128]{1,0:T(8,128)(2,1)S(1)}, u32[]{:S(2)}, u32[]{:S(2)}) collective-permute-start(bf16[384,128]{1,0:T(8,128)(2,1)} %get-tuple-element.47.later_ref), channel_id=1, source_target_pairs={{0,32},{32,64},{64,96},{96,128},{128,160},{160,192},{192,224},{1,3... | collective-permute-start | bytes 294920 | tf_op jit(solution)/shard_map/ppermute | solution.py:349
  43.3 8.2 %collective-permute-start.4 = (bf16[384,128]{1,0:T(8,128)(2,1)}, bf16[384,128]{1,0:T(8,128)(2,1)S(1)}, u32[]{:S(2)}, u32[]{:S(2)}) collective-permute-start(bf16[384,128]{1,0:T(8,128)(2,1)} %join_one.1.through_ref), channel_id=1, source_target_pairs={{0,64},{32,96},{64,128},{96,160},{128,192},{160,224},{1,65},{33,97... | collective-permute-start | bytes 294920 | tf_op jit(solution)/shard_map/ppermute | solution.py:349
  53.9 15.8 %collective-permute-start.5 = (bf16[192,128]{1,0:T(8,128)(2,1)}, bf16[192,128]{1,0:T(8,128)(2,1)S(1)}, u32[]{:S(2)}, u32[]{:S(2)}) collective-permute-start(bf16[192,128]{1,0:T(8,128)(2,1)} %get-tuple-element.48), channel_id=1, source_target_pairs={{0,128},{32,160},{64,192},{96,224},{1,129},{33,161},{65,193},{97,2... | collective-permute-start | bytes 147464 | tf_op jit(solution)/shard_map/ppermute | solution.py:349
  95.9 12.1 %collective-permute-start.8 = (bf16[96,2048]{1,0:T(8,128)(2,1)}, bf16[96,2048]{1,0:T(8,128)(2,1)S(1)}, u32[]{:S(2)}, u32[]{:S(2)}) collective-permute-start(bf16[96,2048]{1,0:T(8,128)(2,1)} %project.1.mine_ref), channel_id=1, source_target_pairs={{0,2},{2,4},{4,6},{6,0},{1,3},{3,5},{5,7},{7,1},{8,10},{10,12},{12... | collective-permute-start | bytes 1179656 | tf_op jit(solution)/shard_map/ppermute | solution.py:349
  96.5 11.6 %collective-permute-start.9 = (bf16[96,2048]{1,0:T(8,128)(2,1)}, bf16[96,2048]{1,0:T(8,128)(2,1)S(1)}, u32[]{:S(2)}, u32[]{:S(2)}) collective-permute-start(bf16[96,2048]{1,0:T(8,128)(2,1)} %project.1.mine_ref), channel_id=1, source_target_pairs={{0,6},{2,0},{4,2},{6,4},{1,7},{3,1},{5,3},{7,5},{8,14},{10,8},{12,... | collective-permute-start | bytes 1179656 | tf_op jit(solution)/shard_map/ppermute | solution.py:349
  108.0 7.0 %collective-permute-start.13 = (bf16[48,2048]{1,0:T(8,128)(2,1)S(1)}, bf16[48,2048]{1,0:T(8,128)(2,1)S(1)}, u32[]{:S(2)}, u32[]{:S(2)}) collective-permute-start(bf16[48,2048]{1,0:T(8,128)(2,1)S(1)} %slice.58), channel_id=1, source_target_pairs={{0,2},{2,4},{4,6},{6,0},{1,3},{3,5},{5,7},{7,1},{8,10},{10,12},{12... | collective-permute-start | bytes 589832 | tf_op jit(solution)/shard_map/ppermute | solution.py:349
  108.2 6.9 %collective-permute-start.14 = (bf16[48,2048]{1,0:T(8,128)(2,1)S(1)}, bf16[48,2048]{1,0:T(8,128)(2,1)S(1)}, u32[]{:S(2)}, u32[]{:S(2)}) collective-permute-start(bf16[48,2048]{1,0:T(8,128)(2,1)S(1)} %slice.59), channel_id=1, source_target_pairs={{0,6},{2,0},{4,2},{6,4},{1,7},{3,1},{5,3},{7,5},{8,14},{10,8},{12,... | collective-permute-start | bytes 589832 | tf_op jit(solution)/shard_map/ppermute | solution.py:349
  111.5 12.8 %copy-start.6 = (bf16[192,2048]{1,0:T(8,128)(2,1)}, bf16[192,2048]{1,0:T(8,128)(2,1)S(1)}, u32[]{:S(2)}) copy-start(bf16[192,2048]{1,0:T(8,128)(2,1)S(1)} %constant_dynamic-update-slice_fusion.mine_ref) | copy-start | bytes 2359300
  111.5 13.0 %collective-permute-start.10 = (bf16[192,2048]{1,0:T(8,128)(2,1)S(1)}, bf16[192,2048]{1,0:T(8,128)(2,1)S(1)}, u32[]{:S(2)}, u32[]{:S(2)}) collective-permute-start(bf16[192,2048]{1,0:T(8,128)(2,1)S(1)} %constant_dynamic-update-slice_fusion.mine_ref), channel_id=1, source_target_pairs={{0,1},{1,0},{2,3},{3,2},{4,5},{5,4},{6,7},{7,6},{8,9},{9,8},{10,11... | collective-permute-start | bytes 2359304 | tf_op jit(solution)/shard_map/ppermute | solution.py:491
  115.1 1.8 %copy-start = (bf16[96,2048]{1,0:T(8,128)(2,1)}, bf16[96,2048]{1,0:T(8,128)(2,1)S(1)}, u32[]{:S(2)}) copy-start(bf16[96,2048]{1,0:T(8,128)(2,1)S(1)} %constant_dynamic-update-slice_fusion.2.mine_ref) | copy-start | bytes 1179652
  115.1 1.8 %collective-permute-start.15 = (bf16[96,2048]{1,0:T(8,128)(2,1)S(1)}, bf16[96,2048]{1,0:T(8,128)(2,1)S(1)}, u32[]{:S(2)}, u32[]{:S(2)}) collective-permute-start(bf16[96,2048]{1,0:T(8,128)(2,1)S(1)} %constant_dynamic-update-slice_fusion.2.mine_ref), channel_id=1, source_target_pairs={{0,1},{1,0},{2,3},{3,2},{4,5},{5,4},{6,7},{7,6},{8,9},{9,8},{10,11... | collective-permute-start | bytes 1179656 | tf_op jit(solution)/shard_map/ppermute | solution.py:491
  124.3 9.9 %copy-start.4 = (bf16[96,2048]{1,0:T(8,128)(2,1)S(1)}, bf16[96,2048]{1,0:T(8,128)(2,1)}, u32[]{:S(2)}) copy-start(bf16[96,2048]{1,0:T(8,128)(2,1)} %get-tuple-element.63) | copy-start | bytes 1179652
  124.3 9.9 %collective-permute-start.16 = (bf16[96,2048]{1,0:T(8,128)(2,1)}, bf16[96,2048]{1,0:T(8,128)(2,1)S(1)}, u32[]{:S(2)}, u32[]{:S(2)}) collective-permute-start(bf16[96,2048]{1,0:T(8,128)(2,1)} %get-tuple-element.64), channel_id=1, source_target_pairs={{0,1},{1,0},{2,3},{3,2},{4,5},{5,4},{6,7},{7,6},{8,9},{9,8},{10,11... | collective-permute-start | bytes 1179656 | tf_op jit(solution)/shard_map/ppermute | solution.py:491
  133.6 12.2 %collective-permute-start.11 = (bf16[192,2048]{1,0:T(8,128)(2,1)}, bf16[192,2048]{1,0:T(8,128)(2,1)S(1)}, u32[]{:S(2)}, u32[]{:S(2)}) collective-permute-start(bf16[192,2048]{1,0:T(8,128)(2,1)} %get-tuple-element.62), channel_id=1, source_target_pairs={{0,1},{1,0},{2,3},{3,2},{4,5},{5,4},{6,7},{7,6},{8,9},{9,8},{10,11... | collective-permute-start | bytes 2359304 | tf_op jit(solution)/shard_map/ppermute | solution.py:491
  134.0 3.6 %collective-permute-start.6 = (bf16[96,2048]{1,0:T(8,128)(2,1)}, bf16[96,2048]{1,0:T(8,128)(2,1)S(1)}, u32[]{:S(2)}, u32[]{:S(2)}) collective-permute-start(bf16[96,2048]{1,0:T(8,128)(2,1)} %project.1.mine_ref), channel_id=1, source_target_pairs={{0,1},{1,0},{2,3},{3,2},{4,5},{5,4},{6,7},{7,6},{8,9},{9,8},{10,11... | collective-permute-start | bytes 1179656 | tf_op jit(solution)/shard_map/ppermute | solution.py:491
  134.3 11.0 %collective-permute-start.17 = (bf16[48,2048]{1,0:T(8,128)(2,1)S(1)}, bf16[48,2048]{1,0:T(8,128)(2,1)S(1)}, u32[]{:S(2)}, u32[]{:S(2)}) collective-permute-start(bf16[48,2048]{1,0:T(8,128)(2,1)S(1)} %get-tuple-element.71), channel_id=1, source_target_pairs={{0,6},{2,0},{4,2},{6,4},{1,7},{3,1},{5,3},{7,5},{8,14},{10,8},{12,... | collective-permute-start | bytes 589832 | tf_op jit(solution)/shard_map/ppermute | solution.py:349
  137.7 8.1 %copy-start.1 = (bf16[192,2048]{1,0:T(8,128)(2,1)S(1)}, bf16[192,2048]{1,0:T(8,128)(2,1)}, u32[]{:S(2)}) copy-start(bf16[192,2048]{1,0:T(8,128)(2,1)} %get-tuple-element.61) | copy-start | bytes 2359300
  137.7 8.1 %collective-permute-start.19 = (bf16[48,2048]{1,0:T(8,128)(2,1)S(1)}, bf16[48,2048]{1,0:T(8,128)(2,1)S(1)}, u32[]{:S(2)}, u32[]{:S(2)}) collective-permute-start(bf16[48,2048]{1,0:T(8,128)(2,1)S(1)} %get-tuple-element.72), channel_id=1, source_target_pairs={{0,2},{2,4},{4,6},{6,0},{1,3},{3,5},{5,7},{7,1},{8,10},{10,12},{12... | collective-permute-start | bytes 589832 | tf_op jit(solution)/shard_map/ppermute | solution.py:349
  145.1 18.3 %copy-start.11 = (f32[2048]{0:T(1024)S(1)}, f32[2048]{0:T(1024)}, u32[]{:S(2)}) copy-start(f32[2048]{0:T(1024)} %param.49) | copy-start | bytes 24580
  145.1 6.1 %collective-permute-start.7 = (bf16[96,2048]{1,0:T(8,128)(2,1)}, bf16[96,2048]{1,0:T(8,128)(2,1)S(1)}, u32[]{:S(2)}, u32[]{:S(2)}) collective-permute-start(bf16[96,2048]{1,0:T(8,128)(2,1)} %get-tuple-element.60), channel_id=1, source_target_pairs={{0,1},{1,0},{2,3},{3,2},{4,5},{5,4},{6,7},{7,6},{8,9},{9,8},{10,11... | collective-permute-start | bytes 1179656 | tf_op jit(solution)/shard_map/ppermute | solution.py:491
  146.1 8.3 %collective-permute-start.12 = (bf16[48,2048]{1,0:T(8,128)(2,1)S(1)}, bf16[48,2048]{1,0:T(8,128)(2,1)S(1)}, u32[]{:S(2)}, u32[]{:S(2)}) collective-permute-start(bf16[48,2048]{1,0:T(8,128)(2,1)S(1)} %get-tuple-element.67), channel_id=1, source_target_pairs={{0,6},{2,0},{4,2},{6,4},{1,7},{3,1},{5,3},{7,5},{8,14},{10,8},{12,... | collective-permute-start | bytes 589832 | tf_op jit(solution)/shard_map/ppermute | solution.py:349
  149.1 9.0 %collective-permute-start.18 = (bf16[48,2048]{1,0:T(8,128)(2,1)S(1)}, bf16[48,2048]{1,0:T(8,128)(2,1)S(1)}, u32[]{:S(2)}, u32[]{:S(2)}) collective-permute-start(bf16[48,2048]{1,0:T(8,128)(2,1)S(1)} %get-tuple-element.70), channel_id=1, source_target_pairs={{0,6},{2,0},{4,2},{6,4},{1,7},{3,1},{5,3},{7,5},{8,14},{10,8},{12,... | collective-permute-start | bytes 589832 | tf_op jit(solution)/shard_map/ppermute | solution.py:349
  149.2 9.0 %collective-permute-start.20 = (bf16[48,2048]{1,0:T(8,128)(2,1)S(1)}, bf16[48,2048]{1,0:T(8,128)(2,1)S(1)}, u32[]{:S(2)}, u32[]{:S(2)}) collective-permute-start(bf16[48,2048]{1,0:T(8,128)(2,1)S(1)} %get-tuple-element.69), channel_id=1, source_target_pairs={{0,2},{2,4},{4,6},{6,0},{1,3},{3,5},{5,7},{7,1},{8,10},{10,12},{12... | collective-permute-start | bytes 589832 | tf_op jit(solution)/shard_map/ppermute | solution.py:349
  151.1 10.5 %collective-permute-start.21 = (bf16[48,2048]{1,0:T(8,128)(2,1)S(1)}, bf16[48,2048]{1,0:T(8,128)(2,1)S(1)}, u32[]{:S(2)}, u32[]{:S(2)}) collective-permute-start(bf16[48,2048]{1,0:T(8,128)(2,1)S(1)} %get-tuple-element.68), channel_id=1, source_target_pairs={{0,2},{2,4},{4,6},{6,0},{1,3},{3,5},{5,7},{7,1},{8,10},{10,12},{12... | collective-permute-start | bytes 589832 | tf_op jit(solution)/shard_map/ppermute | solution.py:349
  (9 other events, 8.0 us)
Sparse Core Ops, SparseCore 0:
  9.9 100.9 all-gather.2

commit v2 on v1

--- a/solution.py
+++ b/solution.py
@@ -5,6 +5,7 @@
 from jax.experimental.pallas import tpu as pltpu
 from jax.sharding import Mesh
 from jax.sharding import PartitionSpec as P
+
 
 CHUNK = 64
 LANES = 128
@@ -205,7 +206,7 @@
 
 def chunk_maps(first, second):
     tokens = first[0].shape[0]
-    block = 256
+    block = 384
     chunks = tokens // CHUNK
     units = 3 * tokens // LANES
     rows = pl.BlockSpec((block, LANES), lambda i: (i, 0))
@@ -234,7 +235,18 @@
     )(*first, *second)
 
 
-def reads_kernel(solved, reads, begin_1, begin_2, v_1, v_2, entry_1, inner_1, entry_2, inner_2):
+def reads_kernel(
+    solved, reads, begin_1, begin_2, v_1, v_2, sq1, sz1, sq2, sz2, entry_1, inner_1, entry_2, inner_2
+):
+    def store(at, entry, inner, sq, sz, entry_out, inner_out):
+        for c in range(entry.shape[0] // CHUNK):
+            part = slice(c * CHUNK, (c + 1) * CHUNK)
+            rows = slice(at + c * CHUNK, at + (c + 1) * CHUNK)
+            n = at // CHUNK + c
+            short = entry[part].astype(BF16)
+            entry_out[rows] = mm_nt(short, sq[n]).astype(BF16)
+            inner_out[rows] = inner[part] + mm_nt(short, sz[n])
+
     for b in range(begin_1.shape[0] // LANES):
         for u in range(3):
             n = 3 * b + u
@@ -246,29 +258,31 @@
             entry = carried[:, :LANES]
             inner = carried[:, LANES:] + mm(reads[n, :, LANES:], value)
             if u == 2:
-                entry_2[at] = (begin_2[at].astype(F32) + entry).astype(BF16)
-                inner_2[at] = inner
+                entry = begin_2[at].astype(F32) + entry
+                store(at.start, entry, inner, sq2, sz2, entry_2, inner_2)
             else:
-                entry_1[at] = (begin_1[at].astype(F32) + entry[:CHUNK] + entry[CHUNK:]).astype(BF16)
-                inner_1[at] = inner[:CHUNK] + inner[CHUNK:]
-
-
-def chunk_reads(solved, reads, begin_1, begin_2, v_1, v_2):
+                entry = begin_1[at].astype(F32) + entry[:CHUNK] + entry[CHUNK:]
+                inner = inner[:CHUNK] + inner[CHUNK:]
+                store(at.start, entry, inner, sq1, sz1, entry_1, inner_1)
+
+
+def chunk_reads(solved, reads, begin_1, begin_2, v_1, v_2, *starts):
     tokens = begin_1.shape[0]
     block = 256
     rows = pl.BlockSpec((block, LANES), lambda i: (i, 0))
     unit = pl.BlockSpec((3 * block // LANES, LANES, 2 * LANES), lambda i: (i, 0, 0))
+    state = pl.BlockSpec((block // CHUNK, LANES, LANES), lambda i: (i, 0, 0))
     return pl.pallas_call(
         reads_kernel,
         grid=(tokens // block,),
-        in_specs=[unit, unit] + [rows] * 4,
+        in_specs=[unit, unit] + [rows] * 4 + [state] * 4,
         out_specs=[rows] * 4,
         out_shape=[jax.ShapeDtypeStruct((tokens, LANES), t) for t in (BF16, F32, BF16, F32)],
         cost_estimate=pl.CostEstimate(
             flops=4_000_000_000, bytes_accessed=6_000_000, transcendentals=0
         ),
         name="chunk_reads",
-    )(solved, reads, begin_1, begin_2, v_1, v_2)
+    )(solved, reads, begin_1, begin_2, v_1, v_2, *starts)
 
 
 def unpack(packed):
@@ -321,14 +335,13 @@
     total_ref[...] = pack(running)
 
 
-def vmem_call(kernel, out_shape, *args, scalars=0, name=None):
+def vmem_call(kernel, out_shape, *args, scalars=0):
     return pl.pallas_call(
         kernel,
         in_specs=[pl.BlockSpec(memory_space=pltpu.SMEM)] * scalars
         + [pl.BlockSpec(memory_space=pltpu.VMEM)] * (len(args) - scalars),
         out_specs=jax.tree.map(lambda _: pl.BlockSpec(memory_space=pltpu.VMEM), out_shape),
         out_shape=out_shape,
-        name=name,
     )(*args)
 
 
@@ -355,22 +368,18 @@
     peers = [shift(total, "y", s, ny, True) for s in (1, 2, 3)]
     peers, entries = lax.optimization_barrier((peers, entries))
     mine = lax.axis_index("y").astype(jnp.int32).reshape(1)
-    row_before, row_total = vmem_call(
-        row_kernel, (shape, shape), mine, total, *peers, scalars=1, name="row_maps"
-    )
+    row_before, row_total = vmem_call(row_kernel, (shape, shape), mine, total, *peers, scalars=1)
     before = shift(row_total, "z", 1, nz, False)
-    through = vmem_call(join_kernel, shape, before, row_total, name="join_one")
+    through = vmem_call(join_kernel, shape, before, row_total)
     earlier = shift(through, "z", 2, nz, False)
     short = jax.ShapeDtypeStruct((192, LANES), BF16)
-    before, send = vmem_call(
-        join_two_kernel, (shape, short), earlier, before, through, name="join_two"
-    )
+    before, send = vmem_call(join_two_kernel, (shape, short), earlier, before, through)
     last = shift(send, "z", 4, nz, False)
     return (last, before, row_before), entries
 
 
 def outputs_kernel(*refs):
-    (last, before, row_before), ins, out, states = refs[:3], refs[3:19], refs[19], refs[20]
+    (last, before, row_before), ins, out, states = refs[:3], refs[3:15], refs[15], refs[16]
 
     @pl.when(pl.program_id(0) == 0)
     def _():
@@ -382,16 +391,10 @@
             states[g] = mm(start, row[g][:LANES]) + row[g][LANES:]
 
     for g in range(2):
-        entry, inner, sq, sz, q_ref, k_ref, v_ref, gate_ref = ins[8 * g : 8 * g + 8]
+        entry, inner, q_ref, k_ref, v_ref, gate_ref = ins[6 * g : 6 * g + 6]
         pair = g == 0
         gain, weight = out_params(refs, g)
-        start = states[g].astype(BF16)
-        pieces = []
-        for c in range(sq.shape[0]):
-            at = slice(c * CHUNK, (c + 1) * CHUNK)
-            state = mm(start, sq[c]) + sz[c]
-            pieces.append(mm_nt(entry[at], state) + inner[at])
-        heady = jnp.concatenate(pieces, 0)
+        heady = mm_nt(entry[...], states[g]) + inner[...]
         q, k, v, gate = (r[...].astype(F32) for r in (q_ref, k_ref, v_ref, gate_ref))
         centred = heady - head_mean(heady, pair)
         spread_ = head_mean(centred * centred, pair)
@@ -404,7 +407,7 @@
 
 
 def out_params(refs, g):
-    params = refs[21]
+    params = refs[17]
     return params[2 * g : 2 * g + 1], params[2 * g + 1 : 2 * g + 2]
 
 
@@ -412,20 +415,19 @@
     tokens = groups[0][0].shape[0]
     block = 256
     rows = pl.BlockSpec((block, LANES), lambda i: (i, 0))
-    state = pl.BlockSpec((block // CHUNK, LANES, LANES), lambda i: (i, 0, 0))
 
     def whole(a):
         return pl.BlockSpec(a.shape, lambda i: (0,) * a.ndim)
 
     def kernel(*refs):
-        ins, out, states = refs[:20], refs[20], refs[21]
-        outputs_kernel(*ins[:19], out, states, ins[19])
+        ins, out, states = refs[:16], refs[16], refs[17]
+        outputs_kernel(*ins[:15], out, states, ins[15])
 
     return pl.pallas_call(
         kernel,
         grid=(tokens // block,),
         in_specs=[whole(a) for a in prefix]
-        + [rows, rows, state, state, rows, rows, rows, rows] * 2
+        + [rows] * 12
         + [whole(params)],
         out_specs=pl.BlockSpec((block, 2 * LANES), lambda i: (i, 0)),
         out_shape=jax.ShapeDtypeStruct((tokens, 2 * LANES), BF16),
@@ -491,8 +493,9 @@
     return lax.ppermute(array, "c", [(0, 1), (1, 0)])
 
 
-def channel_kernel(mine_ref, theirs_ref, weights, mine_out, theirs_out, rows, acc, held, sems):
-    count, width = mine_ref.shape
+def channel_kernel(*refs):
+    blocks, refs = refs[:-9], refs[-9:]
+    weights, outs, (rows, acc, held, sems) = refs[0], refs[1:5], refs[5:]
     pieces, group, depth, _ = held.shape
     half = pieces // 2
     block = group * depth
@@ -504,10 +507,11 @@
         copies.append(pltpu.make_async_copy(side, held.at[n], sems.at[n]))
     for copy in copies:
         copy.start()
-    for n in range(half):
-        at = slice(n * block, (n + 1) * block)
-        rows[n, :count] = mine_ref[:, at]
-        rows[n, count:] = theirs_ref[:, at]
+    start = 0
+    for ref in blocks:
+        for n in range(half):
+            rows[n, start : start + ref.shape[0]] = ref[:, n * block : (n + 1) * block]
+        start += ref.shape[0]
     for n in range(half):
         copies[n].wait()
         part = jnp.dot(rows[n], held[n].reshape(block, -1), preferred_element_type=F32)
@@ -516,26 +520,29 @@
     for n in range(half):
         copies[half + n].wait()
         part = mm_nt(hidden, held[half + n].reshape(block, -1)).astype(BF16)
-        at = slice(n * block, (n + 1) * block)
-        mine_out[:, at] = part[:count]
-        theirs_out[:, at] = part[count:]
-
-
-def channel(mine, theirs, weights):
-    count, width = mine.shape
+        start = 0
+        for out in outs:
+            out[:, n * block : (n + 1) * block] = part[start : start + out.shape[0]]
+            start += out.shape[0]
+
+
+def channel(blocks, weights):
     peers, depth, hidden = weights.shape
+    width = blocks[0].shape[1]
+    count = sum(b.shape[0] for b in blocks) // 2
     pieces = 8
-    group = 2 * peers // pieces
-    rows = pl.BlockSpec(memory_space=pltpu.VMEM)
+    near = pl.BlockSpec(memory_space=pltpu.VMEM)
     return pl.pallas_call(
         channel_kernel,
-        in_specs=[rows, rows, pl.BlockSpec(memory_space=pl.ANY)],
-        out_specs=[rows, rows],
-        out_shape=[jax.ShapeDtypeStruct((count, width), BF16)] * 2,
+        in_specs=[near] * len(blocks) + [pl.BlockSpec(memory_space=pl.ANY)],
+        out_specs=[near] * 4,
+        out_shape=[
+            jax.ShapeDtypeStruct((rows, width), BF16) for rows in (3 * count // 4, count // 4) * 2
+        ],
         scratch_shapes=[
             pltpu.VMEM((pieces // 2, 2 * count, 2 * width // pieces), BF16),
             pltpu.VMEM((2 * count, hidden), F32),
-            pltpu.VMEM((pieces, group, depth // 2, hidden), BF16),
+            pltpu.VMEM((pieces, 2 * peers // pieces, depth // 2, hidden), BF16),
             pltpu.SemaphoreType.DMA((pieces,)),
         ],
         cost_estimate=pl.CostEstimate(
@@ -544,10 +551,10 @@
             transcendentals=0,
         ),
         name="channel",
-    )(mine, theirs, weights)
-
-
-def local(
+    )(*blocks, weights)
+
+
+def layer(
     stream,
     query_first,
     key_first,
@@ -574,7 +581,7 @@
     mixer_down_weight,
     final_norm_gain,
 ):
-    count, width = stream.shape
+    count, _ = stream.shape
     both = jnp.concatenate([mixer_up_weight, mixer_down_weight.T], 0)
     weights = lax.all_gather(both, SP)
 
@@ -589,7 +596,9 @@
             extra_decay_second.T,
         ),
     )
-    entries = chunk_reads(solved, reads, begin_1, begin_2, value_first, value_second)
+    entries = chunk_reads(
+        solved, reads, begin_1, begin_2, value_first, value_second, sq1, sz1, sq2, sz2
+    )
     prefix, (entry_1, inner_1, entry_2, inner_2) = sequence_prefix(total, entries)
     params = jnp.stack(
         [head_norm_gain_first, self_weight_first, head_norm_gain_second, self_weight_second]
@@ -597,8 +606,8 @@
     mixer = mixer_outputs(
         prefix,
         (
-            (entry_1, inner_1, sq1, sz1, query_first, key_first, value_first, output_gate_first),
-            (entry_2, inner_2, sq2, sz2, query_second, key_second, value_second, output_gate_second),
+            (entry_1, inner_1, query_first, key_first, value_first, output_gate_first),
+            (entry_2, inner_2, query_second, key_second, value_second, output_gate_second),
         ),
         params,
     )
@@ -609,41 +618,31 @@
 
     nx = lax.axis_size("x")
     half = count // 2
+    own_there = swap_core(middle)
     near_p = shift(middle, "x", 1, nx, True)
     near_m = shift(middle, "x", -1, nx, True)
     far = jnp.concatenate(
         [shift(near_p[:half], "x", 1, nx, True), shift(near_m[half:], "x", -1, nx, True)], 0
     )
     near = jnp.concatenate([near_p, near_m], 0)
-    own_there = swap_core(middle)
     near_there = swap_core(near)
     far_there = swap_core(far)
-
-    far_part, far_send = channel(far, far_there, weights)
+    near_part, far_part, near_send, far_send = channel(
+        (middle, near, far, own_there, near_there, far_there), weights
+    )
     far_back = swap_core(far_send)
-    near_part, near_send = channel(near, near_there, weights)
     near_back = swap_core(near_send)
-    own_part, own_send = channel(middle, own_there, weights)
-    own_back = swap_core(own_send)
-
-    def total_of(part, back, at, more=None):
-        out = part[at : at + half].astype(F32) + back[at : at + half].astype(F32)
-        if more is not None:
-            out = out + more.astype(F32)
-        return out.astype(BF16)
-
-    from_p = shift(total_of(far_part, far_back, 0), "x", 1, nx, True)
-    from_m = shift(total_of(far_part, far_back, half), "x", -1, nx, True)
-    back_p_first = shift(total_of(near_part, near_back, 0), "x", -1, nx, True)
-    back_m_second = shift(total_of(near_part, near_back, 3 * half), "x", 1, nx, True)
-    back_p_second = shift(total_of(near_part, near_back, half, from_m), "x", -1, nx, True)
-    back_m_first = shift(total_of(near_part, near_back, 2 * half, from_p), "x", 1, nx, True)
-    ff_total = (
-        own_part.astype(F32)
-        + own_back.astype(F32)
-        + jnp.concatenate([back_p_first, back_p_second], 0).astype(F32)
-        + jnp.concatenate([back_m_first, back_m_second], 0).astype(F32)
-    )
+
+    def total_of(part, back, n):
+        at = slice(n * count, (n + 1) * count)
+        return part[at].astype(F32) + back[at].astype(F32)
+
+    from_far = shift(total_of(far_part, far_back, 0).astype(BF16), "x", 2, nx, True)
+    from_p = shift(total_of(near_part, near_back, 1).astype(BF16), "x", -1, nx, True)
+    from_m = shift(total_of(near_part, near_back, 2).astype(BF16), "x", 1, nx, True)
+    ff_total = total_of(near_part, near_back, 0)
+    for part in (from_far, from_p, from_m):
+        ff_total = ff_total + part.astype(F32)
     return norm_rows(ALPHA * middle.astype(F32) + ff_total, final_norm_gain).astype(BF16)
 
 
@@ -652,7 +651,7 @@
     long = P(SP, TP)
     group = (long,) * 7 + (P(TP), P(TP))
     return jax.shard_map(
-        local,
+        layer,
         mesh=split,
         in_specs=(P(ALL, None),)
         + group

time: 172 us -> 164 us (0.953); the launches traced: 171 us -> 161 us
  Pallas kernels: 55.6 us -> 46.1 us
  waiting for transfers between devices: 34.8 us -> 42.1 us
  starting transfers between devices: 43.4 us -> 37 us
    pallas_call x3 -> x1, Pallas kernels: 21.4 us -> 12.7 us  [channel(): pl.pallas_call(channel_kernel, in_specs=[near] * len(blocks) + [pl.BlockS...]
    ppermute x16 -> x13, starting transfers between devices: 42 us -> 36.2 us  [shift(): return lax.ppermute(array, axis, pairs)]
    ppermute x16 -> x13, waiting for transfers between devices: 33.1 us -> 37.3 us  [shift(): return lax.ppermute(array, axis, pairs)]
    ppermute x6 -> x5, waiting for transfers between devices: 1.72 us -> 4.81 us  [swap_core(): return lax.ppermute(array, 'c', [(0, 1), (1, 0)])]
    pallas_call x1, Pallas kernels: 4.01 us -> 6.14 us  [chunk_reads(): pl.pallas_call(reads_kernel, grid=(tokens // block,), in_specs=[unit, uni...]
  transfers between devices with their start and end apart: 23 -> 19, of which waited for: 12 -> 9; matrix products, arithmetic and copies ran while one was open for 1% -> 1% of each run, Pallas kernels for 32% -> 21%
where the time goes in v2:
time: 164 us; the launch traced here: 161 us
  Pallas kernels  46.1 us (28%)
  waiting for transfers between devices  42.1 us (26%)
  starting transfers between devices  37 us (23%)
  between operations  13.7 us (8%)
  blocking collectives  13.3 us (8%)
  other arithmetic  5.33 us (3%)
  local copies, waits for them, and re-layouts  3.66 us (2%)
    ppermute x13, waiting for transfers between devices, shift(): return lax.ppermute(array, axis, pairs)  37.3 us
    ppermute x13, starting transfers between devices, shift(): return lax.ppermute(array, axis, pairs)  36.2 us
    all_to_all x1, blocking collectives, layer(): lax.all_to_all(mixer.reshape(-1, count, 2 * LANES), TP, 0, 0, tiled=True)  13.3 us
    pallas_call x1, Pallas kernels, channel(): pl.pallas_call(channel_kernel, in_specs=[near] * len(blocks) + [pl.BlockS...  12.7 us
    pallas_call x1, Pallas kernels, chunk_maps(): pl.pallas_call(maps_kernel, grid=(tokens // block,), in_specs=ins, out_sp...  10.7 us
    pallas_call x1, Pallas kernels, project(): pl.pallas_call(project_kernel, in_specs=[near, near, near, far, far], out...  6.22 us
    pallas_call x1, Pallas kernels, chunk_reads(): pl.pallas_call(reads_kernel, grid=(tokens // block,), in_specs=[unit, uni...  6.14 us
    pallas_call x3, Pallas kernels, vmem_call(): pl.pallas_call(kernel, in_specs=[pl.BlockSpec(memory_space=pltpu.SMEM)] *...  5.7 us
  transfers between devices with their start and end apart: 19, of which 9 were waited for; matrix products, arithmetic and copies ran while one was open for 1% of the time, Pallas kernels for 21%

profile of v2, /device:TPU:16, one launch (start us, length us, event | category | flops | bytes accessed | tf_op | source)
XLA Modules:
  0.0 161.3 jit_solution(14362193287332352306)
XLA Ops:
  6.5 1.7 %pad_maximum_fusion = bf16[128,1024]{1,0:T(8,128)(2,1)} fusion(bf16[64,1024]{1,0:T(8,128)(2,1)} %bitcast.12, bf16[64,1024]{1,0:T(8,128)(2,1)} %param.47), kind=kLoop, calls=%fused_computation.6 | loop fusion | flops 524288 | bytes 524288 | tf_op jit(solution)/shard_map/concatenate | solution.py:585
  8.2 10.7 %chunk_maps.1 = (bf16[18,128,256]{2,1,0:T(8,128)(2,1)}, bf16[18,128,256]{2,1,0:T(8,128)(2,1)}, bf16[768,128]{1,0:T(8,128)(2,1)}, bf16[768,128]{1,0:T(8,128)(2,1)...) custom-call(bf16[768,128]{1,0:T(8,128)(2,1)} %refs_5_.1, ...), custom_call_target="tpu_custom_call" | custom-call | flops 12000000000 | bytes 8000000 | tf_op jit(solution)/shard_map/chunk_maps/pallas_call | solution.py:218
  18.9 1.4 collective-permute-start
  20.3 0.9 collective-permute-start.1
  21.2 2.5 %collective-permute-start.2 = (bf16[384,128]{1,0:T(8,128)(2,1)}, bf16[384,128]{1,0:T(8,128)(2,1)S(1)}, u32[]{:S(2)}, u32[]{:S(2)}) collective-permute-start(bf16[384,128]{1,0:T(8,128)(2,1)} %get-tuple-element.33.own), channel_id=1, source_target_pairs={{0,24},{8,0},{16,8},{24,16},{1,25},{9,1},{17,9},{25,17},{2,26},{10... | collective-permute-start | bytes 294920 | tf_op jit(solution)/shard_map/ppermute | solution.py:362
  23.7 6.1 %chunk_reads.1 = (bf16[768,128]{1,0:T(8,128)(2,1)}, f32[768,128]{1,0:T(8,128)}, bf16[768,128]{1,0:T(8,128)(2,1)}, f32[768,128]{1,0:T(8,128)}) custom-call(bf16[18,128,256]{2,1,0:T(8,128)(2,1)} %get-tuple-element.34.solved, bf16[18,128,256]{2,1,0:T(8,128)(2,1)} %get-tuple-element.35.reads, bf16[768,128]{1,0:T(8,128)(2,1)} %get-tuple-element.36.begin_1, ...), custom_call_target="tpu_custom_call" | custom-call | flops 4000000000 | bytes 6000000 | tf_op jit(solution)/shard_map/chunk_reads/pallas_call | solution.py:275
  30.6 2.1 %shard_map.235 = (bf16[384,128]{1,0:T(8,128)(2,1)}, bf16[384,128]{1,0:T(8,128)(2,1)}) custom-call(s32[1]{0:T(128)} %bitcast.mine_ref, bf16[384,128]{1,0:T(8,128)(2,1)} %get-tuple-element.33.own, bf16[384,128]{1,0:T(8,128)(2,1)} %copy-done.5, bf16[384,128]{1,0:T(8,128)(2,1)} %copy-done.6, bf16[384,128]{1,0:T(8,128)(2,1)} %copy-done.7), custom_call_target="tpu_custom_call" | custom-call | tf_op jit(solution)/shard_map/pallas_call | solution.py:339
  32.7 2.3 %collective-permute-start.3 = (bf16[384,128]{1,0:T(8,128)(2,1)}, bf16[384,128]{1,0:T(8,128)(2,1)S(1)}, u32[]{:S(2)}, u32[]{:S(2)}) collective-permute-start(bf16[384,128]{1,0:T(8,128)(2,1)} %get-tuple-element.49.later_ref), channel_id=1, source_target_pairs={{0,32},{32,64},{64,96},{96,128},{128,160},{160,192},{192,224},{1,3... | collective-permute-start | bytes 294920 | tf_op jit(solution)/shard_map/ppermute | solution.py:362
  34.9 3.1 %collective-permute-done.3.earlier_ref.before_ref = bf16[384,128]{1,0:T(8,128)(2,1)S(1)} collective-permute-done((bf16[384,128]{1,0:T(8,128)(2,1)}, bf16[384,128]{1,0:T(8,128)(2,1)S(1)}, u32[]{:S(2)}, u32[]{:S(2)}) %collective-permute-start.3) | collective-permute-done | bytes 98336 | tf_op jit(solution)/shard_map/ppermute | solution.py:362
  38.7 1.7 %shard_map.236.through_ref = bf16[384,128]{1,0:T(8,128)(2,1)} custom-call(bf16[384,128]{1,0:T(8,128)(2,1)} %copy-done.1, bf16[384,128]{1,0:T(8,128)(2,1)} %get-tuple-element.49.later_ref), custom_call_target="tpu_custom_call" | custom-call | tf_op jit(solution)/shard_map/pallas_call | solution.py:339
  40.5 6.4 %collective-permute-start.4 = (bf16[384,128]{1,0:T(8,128)(2,1)}, bf16[384,128]{1,0:T(8,128)(2,1)S(1)}, u32[]{:S(2)}, u32[]{:S(2)}) collective-permute-start(bf16[384,128]{1,0:T(8,128)(2,1)} %shard_map.236.through_ref), channel_id=1, source_target_pairs={{0,64},{32,96},{64,128},{96,160},{128,192},{160,224},{1,65},{33,97... | collective-permute-start | bytes 294920 | tf_op jit(solution)/shard_map/ppermute | solution.py:362
  46.9 2.6 %collective-permute-done.4.earlier_ref = bf16[384,128]{1,0:T(8,128)(2,1)S(1)} collective-permute-done((bf16[384,128]{1,0:T(8,128)(2,1)}, bf16[384,128]{1,0:T(8,128)(2,1)S(1)}, u32[]{:S(2)}, u32[]{:S(2)}) %collective-permute-start.4) | collective-permute-done | bytes 98336 | tf_op jit(solution)/shard_map/ppermute | solution.py:362
  50.1 1.8 %shard_map.237 = (bf16[384,128]{1,0:T(8,128)(2,1)}, bf16[192,128]{1,0:T(8,128)(2,1)}) custom-call(bf16[384,128]{1,0:T(8,128)(2,1)} %copy-done.8, bf16[384,128]{1,0:T(8,128)(2,1)} %copy-done.1, bf16[384,128]{1,0:T(8,128)(2,1)} %shard_map.236.through_ref), custom_call_target="tpu_custom_call" | custom-call | tf_op jit(solution)/shard_map/pallas_call | solution.py:339
  52.0 11.5 %collective-permute-start.5 = (bf16[192,128]{1,0:T(8,128)(2,1)}, bf16[192,128]{1,0:T(8,128)(2,1)S(1)}, u32[]{:S(2)}, u32[]{:S(2)}) collective-permute-start(bf16[192,128]{1,0:T(8,128)(2,1)} %get-tuple-element.50), channel_id=1, source_target_pairs={{0,128},{32,160},{64,192},{96,224},{1,129},{33,161},{65,193},{97,2... | collective-permute-start | bytes 147464 | tf_op jit(solution)/shard_map/ppermute | solution.py:362
  64.1 2.3 %collective-permute-done.5.refs_0_ = bf16[192,128]{1,0:T(8,128)(2,1)S(1)} collective-permute-done((bf16[192,128]{1,0:T(8,128)(2,1)}, bf16[192,128]{1,0:T(8,128)(2,1)S(1)}, u32[]{:S(2)}, u32[]{:S(2)}) %collective-permute-start.5) | collective-permute-done | bytes 49184 | tf_op jit(solution)/shard_map/ppermute | solution.py:362
  67.0 4.7 %mixer_outputs.1 = bf16[768,256]{1,0:T(8,128)(2,1)} custom-call(bf16[192,128]{1,0:T(8,128)(2,1)} %copy-done.17, bf16[384,128]{1,0:T(8,128)(2,1)} %get-tuple-element.51.refs_1_, bf16[384,128]{1,0:T(8,128)(2,1)} %get-tuple-element.52.refs_2_, bf16[768,128]{1,0:T(8,128)(2,1)} %get-tuple-element.53.refs_3_, f32[768,128]{1,0:T(8,128)} %get-tuple-element.54.refs_4_, ...), custom_call_target="tpu_custom_call" | custom-call | flops 2000000000 | bytes 6000000 | tf_op jit(solution)/shard_map/mixer_outputs/pallas_call | solution.py:426
  71.7 13.3 %all_to_all.5.rows_ref = bf16[8,96,256]{2,1,0:T(8,128)(2,1)} all-to-all(bf16[8,96,256]{2,1,0:T(8,128)(2,1)} %bitcast.11), channel_id=1, replica_groups=mesh['z'=8,'y'=4,'x'=4,'c'=2] {'x','c'}, dimensions={0} | all-to-all | bytes 786432 | tf_op jit(solution)/shard_map/all_to_all | solution.py:614
  85.0 6.2 %project.1.refs_0_ = bf16[96,2048]{1,0:T(8,128)(2,1)} custom-call(bf16[8,96,256]{2,1,0:T(8,128)(2,1)} %all_to_all.5.rows_ref, bf16[96,2048]{1,0:T(8,128)(2,1)} %stream_ref.1, f32[1,2048]{1,0:T(1,128)} %bitcast.18, bf16[1024,2048]{1,0:T(8,128)(2,1)} %first.1, bf16[1024,2048]{1,0:T(8,128)(2,1)} %second.1), custom_call_target="tpu_custom_call" | custom-call | flops 4000000000 | bytes 9000000 | tf_op jit(solution)/shard_map/project/pallas_call | solution.py:476
  91.9 2.7 %collective-permute-start.7 = (bf16[96,2048]{1,0:T(8,128)(2,1)}, bf16[96,2048]{1,0:T(8,128)(2,1)S(1)}, u32[]{:S(2)}, u32[]{:S(2)}) collective-permute-start(bf16[96,2048]{1,0:T(8,128)(2,1)} %project.1.refs_0_), channel_id=1, source_target_pairs={{0,6},{2,0},{4,2},{6,4},{1,7},{3,1},{5,3},{7,5},{8,14},{10,8},{12,... | collective-permute-start | bytes 1179656 | tf_op jit(solution)/shard_map/ppermute | solution.py:362
  94.6 8.7 %collective-permute-done.6 = bf16[96,2048]{1,0:T(8,128)(2,1)S(1)} collective-permute-done((bf16[96,2048]{1,0:T(8,128)(2,1)}, bf16[96,2048]{1,0:T(8,128)(2,1)S(1)}, u32[]{:S(2)}, u32[]{:S(2)}) %collective-permute-start.6) | collective-permute-done | bytes 393248 | tf_op jit(solution)/shard_map/ppermute | solution.py:362
  103.7 3.3 %collective-permute-start.9 = (bf16[48,2048]{1,0:T(8,128)(2,1)S(1)}, bf16[48,2048]{1,0:T(8,128)(2,1)S(1)}, u32[]{:S(2)}, u32[]{:S(2)}) collective-permute-start(bf16[48,2048]{1,0:T(8,128)(2,1)S(1)} %slice.33), channel_id=1, source_target_pairs={{0,6},{2,0},{4,2},{6,4},{1,7},{3,1},{5,3},{7,5},{8,14},{10,8},{12,... | collective-permute-start | bytes 589832 | tf_op jit(solution)/shard_map/ppermute | solution.py:362
  107.1 3.4 %collective-permute-done.8 = bf16[48,2048]{1,0:T(8,128)(2,1)S(1)} collective-permute-done((bf16[48,2048]{1,0:T(8,128)(2,1)S(1)}, bf16[48,2048]{1,0:T(8,128)(2,1)S(1)}, u32[]{:S(2)}, u32[]{:S(2)}) %collective-permute-start.8) | collective-permute-done | bytes 196640 | tf_op jit(solution)/shard_map/ppermute | solution.py:362
  110.7 1.7 %collective-permute-done.12.refs_5_ = bf16[96,2048]{1,0:T(8,128)(2,1)S(1)} collective-permute-done((bf16[96,2048]{1,0:T(8,128)(2,1)S(1)}, bf16[96,2048]{1,0:T(8,128)(2,1)S(1)}, u32[]{:S(2)}, u32[]{:S(2)}) %collective-permute-start.12) | collective-permute-done | bytes 393248 | tf_op jit(solution)/shard_map/ppermute | solution.py:493
  113.4 12.7 %channel.1 = (bf16[288,2048]{1,0:T(8,128)(2,1)}, bf16[96,2048]{1,0:T(8,128)(2,1)}, bf16[288,2048]{1,0:T(8,128)(2,1)}, bf16[96,2048]{1,0:T(8,128)(2,1)}) custom-call(bf16[96,2048]{1,0:T(8,128)(2,1)} %project.1.refs_0_, bf16[192,2048]{1,0:T(8,128)(2,1)} %copy-done.3, bf16[96,2048]{1,0:T(8,128)(2,1)} %copy-done.4, bf16[96,2048]{1,0:T(8,128)(2,1)} %copy-done.15, ...), custom_call_target="tpu_custom_call" | custom-call | flops 6442450944 | bytes 8388608 | tf_op jit(solution)/shard_map/channel/pallas_call | solution.py:535
  126.7 3.1 %collective-permute-done.14 = bf16[96,2048]{1,0:T(8,128)(2,1)S(1)} collective-permute-done((bf16[96,2048]{1,0:T(8,128)(2,1)}, bf16[96,2048]{1,0:T(8,128)(2,1)S(1)}, u32[]{:S(2)}, u32[]{:S(2)}) %collective-permute-start.14) | collective-permute-done | bytes 393248 | tf_op jit(solution)/shard_map/ppermute | solution.py:493
  129.8 1.1 add_convert_fusion.2
  130.9 1.6 %collective-permute-start.15 = (bf16[96,2048]{1,0:T(8,128)(2,1)S(1)}, bf16[96,2048]{1,0:T(8,128)(2,1)S(1)}, u32[]{:S(2)}, u32[]{:S(2)}) collective-permute-start(bf16[96,2048]{1,0:T(8,128)(2,1)S(1)} %add_convert_fusion.2), channel_id=1, source_target_pairs={{0,4},{2,6},{4,0},{6,2},{1,5},{3,7},{5,1},{7,3},{8,12},{10,14},{12... | collective-permute-start | bytes 1179656 | tf_op jit(solution)/shard_map/ppermute | solution.py:362
  132.8 1.9 %collective-permute-start.16 = (bf16[96,2048]{1,0:T(8,128)(2,1)S(1)}, bf16[96,2048]{1,0:T(8,128)(2,1)S(1)}, u32[]{:S(2)}, u32[]{:S(2)}) collective-permute-start(bf16[96,2048]{1,0:T(8,128)(2,1)S(1)} %get-tuple-element.63), channel_id=1, source_target_pairs={{0,6},{2,0},{4,2},{6,4},{1,7},{3,1},{5,3},{7,5},{8,14},{10,8},{12,... | collective-permute-start | bytes 1179656 | tf_op jit(solution)/shard_map/ppermute | solution.py:362
  134.7 0.9 collective-permute-start.17
  135.6 8.9 %collective-permute-done.15 = bf16[96,2048]{1,0:T(8,128)(2,1)S(1)} collective-permute-done((bf16[96,2048]{1,0:T(8,128)(2,1)S(1)}, bf16[96,2048]{1,0:T(8,128)(2,1)S(1)}, u32[]{:S(2)}, u32[]{:S(2)}) %collective-permute-start.15) | collective-permute-done | bytes 393248 | tf_op jit(solution)/shard_map/ppermute | solution.py:362
  144.5 8.2 %collective-permute-done.16 = bf16[96,2048]{1,0:T(8,128)(2,1)S(1)} collective-permute-done((bf16[96,2048]{1,0:T(8,128)(2,1)S(1)}, bf16[96,2048]{1,0:T(8,128)(2,1)S(1)}, u32[]{:S(2)}, u32[]{:S(2)}) %collective-permute-start.16) | collective-permute-done | bytes 393248 | tf_op jit(solution)/shard_map/ppermute | solution.py:362
  153.5 0.9 multiply_convert_fusion
  (67 shorter events, 7.0 us)
Async XLA Ops:
  6.5 105.8 %all-gather.3.cloned.1.call-start = ((), (), s32[]{:S(2)}) async-start(), calls=%async_computation.1 | async-start | bytes 8650752 | tf_op jit(solution)/shard_map/all_gather | solution.py:586
  18.9 10.9 %collective-permute-start = (bf16[384,128]{1,0:T(8,128)(2,1)}, bf16[384,128]{1,0:T(8,128)(2,1)S(1)}, u32[]{:S(2)}, u32[]{:S(2)}) collective-permute-start(bf16[384,128]{1,0:T(8,128)(2,1)} %get-tuple-element.33.own), channel_id=1, source_target_pairs={{0,8},{8,16},{16,24},{24,0},{1,9},{9,17},{17,25},{25,1},{2,10},{10... | collective-permute-start | bytes 294920 | tf_op jit(solution)/shard_map/ppermute | solution.py:362
  20.3 9.6 %collective-permute-start.1 = (bf16[384,128]{1,0:T(8,128)(2,1)}, bf16[384,128]{1,0:T(8,128)(2,1)S(1)}, u32[]{:S(2)}, u32[]{:S(2)}) collective-permute-start(bf16[384,128]{1,0:T(8,128)(2,1)} %get-tuple-element.33.own), channel_id=1, source_target_pairs={{0,16},{8,24},{16,0},{24,8},{1,17},{9,25},{17,1},{25,9},{2,18},{10... | collective-permute-start | bytes 294920 | tf_op jit(solution)/shard_map/ppermute | solution.py:362
  21.2 8.7 %collective-permute-start.2 = (bf16[384,128]{1,0:T(8,128)(2,1)}, bf16[384,128]{1,0:T(8,128)(2,1)S(1)}, u32[]{:S(2)}, u32[]{:S(2)}) collective-permute-start(bf16[384,128]{1,0:T(8,128)(2,1)} %get-tuple-element.33.own), channel_id=1, source_target_pairs={{0,24},{8,0},{16,8},{24,16},{1,25},{9,1},{17,9},{25,17},{2,26},{10... | collective-permute-start | bytes 294920 | tf_op jit(solution)/shard_map/ppermute | solution.py:362
  23.7 39.8 %copy-start.10 = (f32[128]{0:T(128)S(1)}, f32[128]{0:T(128)}, u32[]{:S(2)}) copy-start(f32[128]{0:T(128)} %param.43) | copy-start | bytes 1540
  23.7 39.8 %copy-start.11 = (f32[128]{0:T(128)S(1)}, f32[128]{0:T(128)}, u32[]{:S(2)}) copy-start(f32[128]{0:T(128)} %param.42) | copy-start | bytes 1540
  23.7 39.8 %copy-start.12 = (f32[128]{0:T(128)S(1)}, f32[128]{0:T(128)}, u32[]{:S(2)}) copy-start(f32[128]{0:T(128)} %param.34) | copy-start | bytes 1540
  23.7 39.8 %copy-start.13 = (f32[128]{0:T(128)S(1)}, f32[128]{0:T(128)}, u32[]{:S(2)}) copy-start(f32[128]{0:T(128)} %param.33) | copy-start | bytes 1540
  29.9 0.7 copy-start.7
  32.7 5.4 %collective-permute-start.3 = (bf16[384,128]{1,0:T(8,128)(2,1)}, bf16[384,128]{1,0:T(8,128)(2,1)S(1)}, u32[]{:S(2)}, u32[]{:S(2)}) collective-permute-start(bf16[384,128]{1,0:T(8,128)(2,1)} %get-tuple-element.49.later_ref), channel_id=1, source_target_pairs={{0,32},{32,64},{64,96},{96,128},{128,160},{160,192},{192,224},{1,3... | collective-permute-start | bytes 294920 | tf_op jit(solution)/shard_map/ppermute | solution.py:362
  40.5 9.0 %collective-permute-start.4 = (bf16[384,128]{1,0:T(8,128)(2,1)}, bf16[384,128]{1,0:T(8,128)(2,1)S(1)}, u32[]{:S(2)}, u32[]{:S(2)}) collective-permute-start(bf16[384,128]{1,0:T(8,128)(2,1)} %shard_map.236.through_ref), channel_id=1, source_target_pairs={{0,64},{32,96},{64,128},{96,160},{128,192},{160,224},{1,65},{33,97... | collective-permute-start | bytes 294920 | tf_op jit(solution)/shard_map/ppermute | solution.py:362
  52.0 14.4 %collective-permute-start.5 = (bf16[192,128]{1,0:T(8,128)(2,1)}, bf16[192,128]{1,0:T(8,128)(2,1)S(1)}, u32[]{:S(2)}, u32[]{:S(2)}) collective-permute-start(bf16[192,128]{1,0:T(8,128)(2,1)} %get-tuple-element.50), channel_id=1, source_target_pairs={{0,128},{32,160},{64,192},{96,224},{1,129},{33,161},{65,193},{97,2... | collective-permute-start | bytes 147464 | tf_op jit(solution)/shard_map/ppermute | solution.py:362
  91.3 12.1 %collective-permute-start.6 = (bf16[96,2048]{1,0:T(8,128)(2,1)}, bf16[96,2048]{1,0:T(8,128)(2,1)S(1)}, u32[]{:S(2)}, u32[]{:S(2)}) collective-permute-start(bf16[96,2048]{1,0:T(8,128)(2,1)} %project.1.refs_0_), channel_id=1, source_target_pairs={{0,2},{2,4},{4,6},{6,0},{1,3},{3,5},{5,7},{7,1},{8,10},{10,12},{12... | collective-permute-start | bytes 1179656 | tf_op jit(solution)/shard_map/ppermute | solution.py:362
  91.9 11.7 %collective-permute-start.7 = (bf16[96,2048]{1,0:T(8,128)(2,1)}, bf16[96,2048]{1,0:T(8,128)(2,1)S(1)}, u32[]{:S(2)}, u32[]{:S(2)}) collective-permute-start(bf16[96,2048]{1,0:T(8,128)(2,1)} %project.1.refs_0_), channel_id=1, source_target_pairs={{0,6},{2,0},{4,2},{6,4},{1,7},{3,1},{5,3},{7,5},{8,14},{10,8},{12,... | collective-permute-start | bytes 1179656 | tf_op jit(solution)/shard_map/ppermute | solution.py:362
  94.6 16.1 %collective-permute-start.10 = (bf16[96,2048]{1,0:T(8,128)(2,1)}, bf16[96,2048]{1,0:T(8,128)(2,1)S(1)}, u32[]{:S(2)}, u32[]{:S(2)}) collective-permute-start(bf16[96,2048]{1,0:T(8,128)(2,1)} %project.1.refs_0_), channel_id=1, source_target_pairs={{0,1},{1,0},{2,3},{3,2},{4,5},{5,4},{6,7},{7,6},{8,9},{9,8},{10,11... | collective-permute-start | bytes 1179656 | tf_op jit(solution)/shard_map/ppermute | solution.py:493
  103.3 7.1 %collective-permute-start.8 = (bf16[48,2048]{1,0:T(8,128)(2,1)S(1)}, bf16[48,2048]{1,0:T(8,128)(2,1)S(1)}, u32[]{:S(2)}, u32[]{:S(2)}) collective-permute-start(bf16[48,2048]{1,0:T(8,128)(2,1)S(1)} %slice.32), channel_id=1, source_target_pairs={{0,2},{2,4},{4,6},{6,0},{1,3},{3,5},{5,7},{7,1},{8,10},{10,12},{12... | collective-permute-start | bytes 589832 | tf_op jit(solution)/shard_map/ppermute | solution.py:362
  103.7 6.9 %collective-permute-start.9 = (bf16[48,2048]{1,0:T(8,128)(2,1)S(1)}, bf16[48,2048]{1,0:T(8,128)(2,1)S(1)}, u32[]{:S(2)}, u32[]{:S(2)}) collective-permute-start(bf16[48,2048]{1,0:T(8,128)(2,1)S(1)} %slice.33), channel_id=1, source_target_pairs={{0,6},{2,0},{4,2},{6,4},{1,7},{3,1},{5,3},{7,5},{8,14},{10,8},{12,... | collective-permute-start | bytes 589832 | tf_op jit(solution)/shard_map/ppermute | solution.py:362
  107.0 5.4 %copy-start.3 = (bf16[192,2048]{1,0:T(8,128)(2,1)}, bf16[192,2048]{1,0:T(8,128)(2,1)S(1)}, u32[]{:S(2)}) copy-start(bf16[192,2048]{1,0:T(8,128)(2,1)S(1)} %constant_dynamic-update-slice_fusion.refs_1_) | copy-start | bytes 2359300
  107.0 5.3 %collective-permute-start.11 = (bf16[192,2048]{1,0:T(8,128)(2,1)S(1)}, bf16[192,2048]{1,0:T(8,128)(2,1)S(1)}, u32[]{:S(2)}, u32[]{:S(2)}) collective-permute-start(bf16[192,2048]{1,0:T(8,128)(2,1)S(1)} %constant_dynamic-update-slice_fusion.refs_1_), channel_id=1, source_target_pairs={{0,1},{1,0},{2,3},{3,2},{4,5},{5,4},{6,7},{7,6},{8,9},{9,8},{10,11... | collective-permute-start | bytes 2359304 | tf_op jit(solution)/shard_map/ppermute | solution.py:493
  110.5 1.9 %copy-start.4 = (bf16[96,2048]{1,0:T(8,128)(2,1)}, bf16[96,2048]{1,0:T(8,128)(2,1)S(1)}, u32[]{:S(2)}) copy-start(bf16[96,2048]{1,0:T(8,128)(2,1)S(1)} %constant_dynamic-update-slice_fusion.2.refs_2_) | copy-start | bytes 1179652
  110.5 1.8 %collective-permute-start.12 = (bf16[96,2048]{1,0:T(8,128)(2,1)S(1)}, bf16[96,2048]{1,0:T(8,128)(2,1)S(1)}, u32[]{:S(2)}, u32[]{:S(2)}) collective-permute-start(bf16[96,2048]{1,0:T(8,128)(2,1)S(1)} %constant_dynamic-update-slice_fusion.2.refs_2_), channel_id=1, source_target_pairs={{0,1},{1,0},{2,3},{3,2},{4,5},{5,4},{6,7},{7,6},{8,9},{9,8},{10,11... | collective-permute-start | bytes 1179656 | tf_op jit(solution)/shard_map/ppermute | solution.py:493
  110.7 1.8 %copy-start.15 = (bf16[96,2048]{1,0:T(8,128)(2,1)}, bf16[96,2048]{1,0:T(8,128)(2,1)S(1)}, u32[]{:S(2)}) copy-start(bf16[96,2048]{1,0:T(8,128)(2,1)S(1)} %collective-permute-done.10.refs_3_) | copy-start | bytes 1179652
  112.4 0.7 copy-start.16
  112.4 1.0 copy-start.14
  126.0 6.4 %copy-start = (bf16[288,2048]{1,0:T(8,128)(2,1)S(1)}, bf16[288,2048]{1,0:T(8,128)(2,1)}, u32[]{:S(2)}) copy-start(bf16[288,2048]{1,0:T(8,128)(2,1)} %get-tuple-element.57) | copy-start | bytes 3538948
  126.1 6.4 %collective-permute-start.13 = (bf16[288,2048]{1,0:T(8,128)(2,1)}, bf16[288,2048]{1,0:T(8,128)(2,1)S(1)}, u32[]{:S(2)}, u32[]{:S(2)}) collective-permute-start(bf16[288,2048]{1,0:T(8,128)(2,1)} %get-tuple-element.58), channel_id=1, source_target_pairs={{0,1},{1,0},{2,3},{3,2},{4,5},{5,4},{6,7},{7,6},{8,9},{9,8},{10,11... | collective-permute-start | bytes 3538952 | tf_op jit(solution)/shard_map/ppermute | solution.py:493
  126.3 3.5 %collective-permute-start.14 = (bf16[96,2048]{1,0:T(8,128)(2,1)}, bf16[96,2048]{1,0:T(8,128)(2,1)S(1)}, u32[]{:S(2)}, u32[]{:S(2)}) collective-permute-start(bf16[96,2048]{1,0:T(8,128)(2,1)} %get-tuple-element.60), channel_id=1, source_target_pairs={{0,1},{1,0},{2,3},{3,2},{4,5},{5,4},{6,7},{7,6},{8,9},{9,8},{10,11... | collective-permute-start | bytes 1179656 | tf_op jit(solution)/shard_map/ppermute | solution.py:493
  130.9 13.6 %collective-permute-start.15 = (bf16[96,2048]{1,0:T(8,128)(2,1)S(1)}, bf16[96,2048]{1,0:T(8,128)(2,1)S(1)}, u32[]{:S(2)}, u32[]{:S(2)}) collective-permute-start(bf16[96,2048]{1,0:T(8,128)(2,1)S(1)} %add_convert_fusion.2), channel_id=1, source_target_pairs={{0,4},{2,6},{4,0},{6,2},{1,5},{3,7},{5,1},{7,3},{8,12},{10,14},{12... | collective-permute-start | bytes 1179656 | tf_op jit(solution)/shard_map/ppermute | solution.py:362
  132.5 20.2 %copy-start.2 = (bf16[96,2048]{1,0:T(8,128)(2,1)S(1)}, bf16[96,2048]{1,0:T(8,128)(2,1)}, u32[]{:S(2)}) copy-start(bf16[96,2048]{1,0:T(8,128)(2,1)} %project.1.refs_0_) | copy-start | bytes 1179652
  132.8 19.9 %collective-permute-start.16 = (bf16[96,2048]{1,0:T(8,128)(2,1)S(1)}, bf16[96,2048]{1,0:T(8,128)(2,1)S(1)}, u32[]{:S(2)}, u32[]{:S(2)}) collective-permute-start(bf16[96,2048]{1,0:T(8,128)(2,1)S(1)} %get-tuple-element.63), channel_id=1, source_target_pairs={{0,6},{2,0},{4,2},{6,4},{1,7},{3,1},{5,3},{7,5},{8,14},{10,8},{12,... | collective-permute-start | bytes 1179656 | tf_op jit(solution)/shard_map/ppermute | solution.py:362
  134.7 18.8 %copy-start.9 = (f32[2048]{0:T(1024)S(1)}, f32[2048]{0:T(1024)}, u32[]{:S(2)}) copy-start(f32[2048]{0:T(1024)} %param.49) | copy-start | bytes 24580
  134.7 18.1 %collective-permute-start.17 = (bf16[96,2048]{1,0:T(8,128)(2,1)S(1)}, bf16[96,2048]{1,0:T(8,128)(2,1)S(1)}, u32[]{:S(2)}, u32[]{:S(2)}) collective-permute-start(bf16[96,2048]{1,0:T(8,128)(2,1)S(1)} %get-tuple-element.64), channel_id=1, source_target_pairs={{0,2},{2,4},{4,6},{6,0},{1,3},{3,5},{5,7},{7,1},{8,10},{10,12},{12... | collective-permute-start | bytes 1179656 | tf_op jit(solution)/shard_map/ppermute | solution.py:362
  (5 other events, 3.2 us)
Sparse Core Ops, SparseCore 0:
  9.9 99.3 all-gather.2
